TPU v7x, 32 devices: a whole 2x2x4 slice. The times are simulated.
32 devices in a mesh: sp: 16 (over z, y, x), tp: 2 (over core).
Axes of the slice: x: 2, y: 2, z: 4, core: 2. Of those that a mesh axis runs over, the one named last changes fastest.
Arguments:
- tokens: bfloat16 [16384, 2048], P(('sp', 'tp')), may hold values from -6 to 6
- norm_gain: float32 [2048], replicated, may hold values from 0.1 to 1.9
- w_query: bfloat16 [2048, 1024], P('sp', 'tp'), may hold values from -0.125 to 0.125
- w_key: bfloat16 [2048, 1024], P('sp', 'tp'), may hold values from -0.125 to 0.125
- w_value: bfloat16 [2048, 1024], P('sp', 'tp'), may hold values from -0.125 to 0.125
- decay_rate: float32 [128, 8], P('sp', 'tp'), may hold values from 3.0517578e-06 to 0.1, as said below
- state_init: float32 [8, 128, 128], P('tp'), may hold values from -48 to 48
- out_gain: float32 [1024], P('tp'), may hold values from 0.1 to 1.9
- w_out: bfloat16 [1024, 2048], P('tp', 'sp'), may hold values from -0.1875 to 0.1875
Outputs:
- mixed: bfloat16 [16384, 2048], P(('sp', 'tp'))
Inputs may be any that keep to these rules, and one draw needn't show every extreme that they name: `decay_rate`: constant over each block of 128 positions.
All inputs are finite; a program needn't handle non-finite values.
Results may differ from a plain program's by a relative error of at most 0.025.
Values may be sent and summed in bfloat16 or wider, within the bound.
A program may use at most 64 MiB of HBM per device.

v0:
```python
import functools

import jax
import jax.numpy as jnp
from jax import lax
from jax.experimental import pallas as pl
from jax.experimental.pallas import tpu as pltpu
from jax.sharding import PartitionSpec as P

HEAD_DIM = 128
BLOCK = 128
EPS = 0.1
ROPE_BASE = 10000.0
MESH = pl.DeviceIdType.MESH
F32 = jnp.float32
BF16 = jnp.bfloat16


def remote(src, dst, send, recv, device):
    return pltpu.make_async_remote_copy(
        src_ref=src, dst_ref=dst, send_sem=send, recv_sem=recv, device_id=device, device_id_type=MESH
    )


class Gather:
    def __init__(self, buf, layers, place, sems):
        self.buf, self.layers, self.place = buf, layers, place
        self.z, self.y, self.x, self.tp = place
        self.rows = buf.shape[0] // (4 * layers)
        self.s_x, self.r_x, self.s_y, self.r_y, self.s_up, self.s_dn, self.r_z = sems

    def at(self, zi, yi, xi, piece=None):
        start = ((zi * 2 + yi) * 2 + xi) * self.rows
        if piece is None:
            return self.buf.at[pl.ds(pl.multiple_of(start, self.rows), self.rows)]
        half = self.rows // 2
        return self.buf.at[pl.ds(pl.multiple_of(start + piece * half, half), half)]

    def device(self, zi, yi, xi):
        return ((zi * 2 + yi) * 2 + xi, self.tp)

    def copy_x(self, zi, j):
        ref = self.at(zi, self.y if j < 2 else 1 - self.y, self.x, (0, 1, 0)[j])
        return remote(ref, ref, self.s_x.at[zi, j], self.r_x.at[zi, j],
                      self.device(self.z, self.y, 1 - self.x))

    def copy_y(self, zi, j):
        ref = self.at(zi, self.y, self.x if j < 2 else 1 - self.x, (1, 0, 1)[j])
        return remote(ref, ref, self.s_y.at[zi, j], self.r_y.at[zi, j],
                      self.device(self.z, 1 - self.y, self.x))

    def copy_z(self, zi, step):
        ref = self.at(zi, self.y, self.x)
        sem = self.s_up if step > 0 else self.s_dn
        return remote(ref, ref, sem.at[zi], self.r_z.at[zi],
                      self.device(self.z + step, self.y, self.x))

    def order(self, t):
        z, last = self.z, self.layers - 1
        near = z - (t + 1) // 2 if t % 2 else z + t // 2
        m = jnp.minimum(z, last - z)
        far = jnp.where(z < last - z, t, last - t)
        return jnp.where(t <= 2 * m, near, far)

    def column(self, t):
        zi = self.order(t)
        if t > 0:
            self.copy_z(zi, 1).wait_recv()
        self.copy_y(zi, 1).start()
        self.copy_x(zi, 1).start()

        @pl.when((zi <= self.z) & (self.z < self.layers - 1))
        def _():
            self.copy_z(zi, 1).start()

        @pl.when((zi >= self.z) & (self.z > 0))
        def _():
            self.copy_z(zi, -1).start()

        self.copy_x(zi, 0).start()
        self.copy_y(zi, 0).start()

    def cross(self, t):
        zi = self.order(t)
        self.copy_y(zi, 1).wait_recv()
        self.copy_x(zi, 2).start()
        self.copy_x(zi, 1).wait_recv()
        self.copy_y(zi, 2).start()

    def arrive(self, t):
        zi = self.order(t)
        for j in (0, 2):
            self.copy_x(zi, j).wait_recv()
            self.copy_y(zi, j).wait_recv()
        return zi

    def drain(self):
        for t in range(self.layers):
            zi = self.order(t)
            for j in range(3):
                self.copy_x(zi, j).wait_send()
                self.copy_y(zi, j).wait_send()

            @pl.when((zi <= self.z) & (self.z < self.layers - 1))
            def _():
                self.copy_z(zi, 1).wait_send()

            @pl.when((zi >= self.z) & (self.z > 0))
            def _():
                self.copy_z(zi, -1).wait_send()


def nt_dot(a, b):
    return lax.dot_general(a, b, (((1,), (1,)), ((), ())), preferred_element_type=F32)


def tn_dot(a, b):
    return lax.dot_general(a, b, (((0,), (0,)), ((), ())), preferred_element_type=F32)


def kernel(layers, peers, tokens, gain, wq, wk, wv, wo, rates, state_init, out_gain, freq, out,
           wkv_all, wq_all, wo_all, normed, acc, cosine, sine, q_rot, k_rot, v_row, inner, prev, state,
           hidden, part, landed, own, tot_send, tot_recv, excl, excl_d, plane_d, z_send, z_recv, incoming,
           local_sem, nrm_s, nrm_r, part_s, part_r, st_s, st_r, zs_s, zs_r, *gather_sems):
    me, tp = lax.axis_index("sp"), lax.axis_index("tp")
    z, y, x = me // 4, (me // 2) % 2, me % 2
    rows_here, width = tokens.shape
    span = rows_here * peers
    cols = wq.shape[1]
    heads = cols // HEAD_DIM
    blocks = span // BLOCK
    shard = wq.shape[0]
    gk = Gather(wkv_all, layers, (z, y, x, tp), gather_sems[:7])
    gq = Gather(wq_all, layers, (z, y, x, tp), gather_sems[7:14])
    go = Gather(wo_all, layers, (z, y, x, tp), gather_sems[14:])

    mine = pl.ds(pl.multiple_of(me * shard, shard), shard)
    fills = [
        pltpu.make_async_copy(src, dst, local_sem.at[i])
        for i, (src, dst) in enumerate((
            (wq, wq_all.at[mine]),
            (wk, wkv_all.at[mine, pl.ds(0, cols)]),
            (wv, wkv_all.at[mine, pl.ds(cols, cols)]),
            (wo, wo_all.at[mine]),
        ))
    ]
    for fill in fills:
        fill.start()

    barrier = pltpu.get_barrier_semaphore()

    def greet(device):
        pl.semaphore_signal(barrier, inc=1, device_id=device, device_id_type=MESH)

    greet(gq.device(z, y, 1 - x))
    greet(gq.device(z, 1 - y, x))
    for d in range(1, peers):
        greet((me, (tp + d) % peers))

    @pl.when(z > 0)
    def _():
        greet(gq.device(z - 1, y, x))

    @pl.when(z < layers - 1)
    def _():
        greet(gq.device(z + 1, y, x))

    pl.semaphore_wait(
        barrier, 1 + peers + jnp.minimum(z, 1) + jnp.minimum(layers - 1 - z, 1))

    for fill in fills:
        fill.wait()
    gk.column(0)

    base = pl.multiple_of(tp * rows_here, rows_here)
    tile = 64

    @pl.loop(0, rows_here // tile)
    def _(i):
        at = pl.ds(pl.multiple_of(i * tile, tile), tile)
        u = tokens[at, :].astype(F32)
        scale = lax.rsqrt(jnp.mean(u * u, axis=-1, keepdims=True) + EPS)
        normed[pl.ds(pl.multiple_of(base + i * tile, tile), tile), :] = (
            u * scale * gain[...]
        ).astype(BF16)

    def send_normed(d):
        ref = normed.at[pl.ds(base, rows_here)]
        return remote(ref, ref, nrm_s.at[d - 1], nrm_r.at[d - 1], (me, (tp + d) % peers))

    def trig(i, carry):
        at = pl.ds(pl.multiple_of(i * BLOCK, BLOCK), BLOCK)
        pos = lax.broadcasted_iota(jnp.int32, (BLOCK, HEAD_DIM), 0) + (me * span + i * BLOCK)
        angle = pos.astype(F32) * freq[...]
        lane = lax.broadcasted_iota(jnp.int32, (BLOCK, HEAD_DIM), 1)
        sin = jnp.sin(angle)
        cosine[at, :] = jnp.cos(angle)
        sine[at, :] = jnp.where(lane < HEAD_DIM // 2, -sin, sin)
        return carry

    for d in range(1, peers):
        send_normed(d).start()
    gk.column(1)
    gk.cross(0)
    if layers > 2:
        gk.column(2)
    for d in range(1, peers):
        send_normed(d).wait_recv()

    deep = 4 * shard
    m_tile = 256

    def product(gather, t, first, count):
        zi = gather.arrive(t)
        at_k = pl.ds(pl.multiple_of(zi * deep, deep), deep)

        @pl.loop(0, span // m_tile)
        def _(i):
            at = pl.ds(pl.multiple_of(i * m_tile, m_tile), m_tile)
            for c in range(count):
                term = jnp.dot(normed[at, at_k], gather.buf[at_k, c * cols:(c + 1) * cols],
                               preferred_element_type=F32)
                at_c = pl.ds((first + c) * cols, cols)
                acc[at, at_c] = term if t == 0 else acc[at, at_c] + term

    cut = [blocks * i // layers for i in range(layers + 1)]
    for t in range(layers):
        lax.fori_loop(cut[t], cut[t + 1], trig, 0)
        if t + 1 < layers:
            gk.cross(t + 1)
        if t + 3 < layers:
            gk.column(t + 3)
        if t == layers - 2:
            gq.column(0)
            gq.column(1)
        product(gk, t, 1, 2)
    gq.cross(0)
    for t in range(2, layers):
        gq.column(t)
        gq.cross(t - 1)

    gap = (lax.broadcasted_iota(jnp.int32, (BLOCK, BLOCK), 0)
           - lax.broadcasted_iota(jnp.int32, (BLOCK, BLOCK), 1)).astype(F32)
    row = lax.broadcasted_iota(jnp.int32, (BLOCK, HEAD_DIM), 0).astype(F32)

    for h in range(heads):
        state[h] = jnp.zeros((HEAD_DIM, HEAD_DIM), F32)

    def states(b, sums):
        at = pl.ds(pl.multiple_of(b * BLOCK, BLOCK), BLOCK)
        cos, sin = cosine[at, :], sine[at, :]
        new = []
        for h in range(heads):
            rate = rates[b, h]
            head = pl.ds(h * HEAD_DIM, HEAD_DIM)
            u = acc[at, pl.ds(cols + h * HEAD_DIM, HEAD_DIM)]
            k = (u * cos + pltpu.roll(u, HEAD_DIM // 2, 1) * sin).astype(BF16)
            v = acc[at, pl.ds(2 * cols + h * HEAD_DIM, HEAD_DIM)].astype(BF16)
            k_rot[at, head] = k
            v_row[at, head] = v
            tail = jnp.exp(-(BLOCK - 1.0 - row) * rate) * HEAD_DIM ** (-0.5)
            kv = tn_dot((k.astype(F32) * tail).astype(BF16), v)
            now = state[h]
            prev[b, h] = now
            state[h] = jnp.exp(jnp.full((1, HEAD_DIM), -float(BLOCK), F32) * rate) * now + kv
            new.append(sums[h] + rate)
        return tuple(new)

    sums = lax.fori_loop(0, blocks, states, (jnp.float32(0.0),) * heads)

    def decay_of(total):
        return jnp.exp(jnp.full((1, HEAD_DIM), -float(BLOCK), F32) * total)

    def pair(step, h, device):
        return remote(tot_send.at[step, h], tot_recv.at[step, h], st_s.at[step, h],
                      st_r.at[step, h], device)

    x_dev, y_dev = gq.device(z, y, 1 - x), gq.device(z, 1 - y, x)
    up_dev = gq.device(z + 1, y, x)

    def put(step, h, decay, value):
        tot_send[step, h, :HEAD_DIM] = value.astype(BF16)
        tot_send[step, h, HEAD_DIM:] = jnp.broadcast_to(decay, (16, HEAD_DIM)).astype(BF16)

    def take(step, h):
        return (tot_recv[step, h, HEAD_DIM:].astype(F32)[:1], tot_recv[step, h, :HEAD_DIM].astype(F32))

    def both(high, decay, value, other):
        d_in, s_in = other
        late = jnp.where(high, decay, d_in)
        total = late * jnp.where(high, s_in, value) + jnp.where(high, value, s_in)
        return decay * d_in, total

    for h in range(heads):
        put(0, h, decay_of(sums[h]), state[h])
        pair(0, h, x_dev).start()

    def inside(b, carry):
        at = pl.ds(pl.multiple_of(b * BLOCK, BLOCK), BLOCK)
        cos, sin = cosine[at, :], sine[at, :]
        for h in range(heads):
            rate = rates[b, h]
            head = pl.ds(h * HEAD_DIM, HEAD_DIM)
            u = acc[at, head]
            q_rot[at, head] = (u * cos + pltpu.roll(u, HEAD_DIM // 2, 1) * sin).astype(BF16)
            fall = jnp.where(gap >= 0.0, jnp.exp(-jnp.maximum(gap, 0.0) * rate), 0.0)
            score = nt_dot(q_rot[at, head], k_rot[at, head]) * (fall * HEAD_DIM ** (-0.5))
            inner[at, head] = jnp.dot(score.astype(BF16), v_row[at, head], preferred_element_type=F32)
        return carry

    gq.cross(layers - 1)
    go.column(0)
    for t in range(layers // 2):
        product(gq, t, 0, 1)
    for h in range(heads):
        pair(0, h, x_dev).wait_recv()
        got = take(0, h)
        excl[h] = jnp.where(x == 1, got[1], 0.0)
        excl_d[h] = jnp.broadcast_to(jnp.where(x == 1, got[0], 1.0), (8, HEAD_DIM))
        decay, value = both(x == 1, decay_of(sums[h]), state[h], got)
        put(1, h, decay, value)
        state[h] = value
        own_decay = jnp.broadcast_to(decay, (8, HEAD_DIM))
        incoming[h, :8] = own_decay
        pair(1, h, y_dev).start()
    go.column(1)
    go.cross(0)
    for t in range(layers // 2, layers):
        product(gq, t, 0, 1)
    for h in range(heads):
        pair(1, h, y_dev).wait_recv()
        got = take(1, h)
        own_d, own_s = excl_d[h][:1], excl[h]
        excl[h] = jnp.where(y == 1, own_d * got[1] + own_s, own_s)
        excl_d[h] = jnp.broadcast_to(jnp.where(y == 1, own_d * got[0], own_d), (8, HEAD_DIM))
        decay, value = both(y == 1, incoming[h, :8][:1], state[h], got)
        state[h] = value
        plane_d[h] = jnp.broadcast_to(decay, (8, HEAD_DIM))

    def lift(h):
        return remote(z_send.at[h], z_recv.at[h], zs_s.at[h], zs_r.at[h], up_dev)

    def relay(from_below):
        for h in range(heads):
            if from_below:
                lift(h).wait_recv()
                incoming[h] = z_recv[h].astype(F32)
            else:
                incoming[h] = state_init[h]

            @pl.when(z < layers - 1)
            def _():
                z_send[h] = (plane_d[h][:1] * incoming[h] + state[h]).astype(BF16)
                lift(h).start()

            incoming[h] = excl_d[h][:1] * incoming[h] + excl[h]

    pl.when(z == 0)(lambda: relay(False))
    if layers > 2:
        go.column(2)
        go.cross(1)
    third = -(-blocks // 3)
    lax.fori_loop(0, third, inside, 0)
    pl.when(z == 1)(lambda: relay(True))
    for t in range(3, layers):
        go.column(t)
        go.cross(t - 1)
    lax.fori_loop(third, 2 * third, inside, 0)
    pl.when(z == 2)(lambda: relay(True))
    go.cross(layers - 1)
    lax.fori_loop(2 * third, blocks, inside, 0)
    pl.when(z > 2)(lambda: relay(True))

    def finish(b, sums):
        at = pl.ds(pl.multiple_of(b * BLOCK, BLOCK), BLOCK)
        new = []
        for h in range(heads):
            rate = rates[b, h]
            head = pl.ds(h * HEAD_DIM, HEAD_DIM)
            before = prev[b, h] + decay_of(sums[h]) * incoming[h]
            read = jnp.exp(-(row + 1.0) * rate)
            kept = inner[at, head] + read * jnp.dot(
                q_rot[at, head], before.astype(BF16), preferred_element_type=F32)
            kept = kept * lax.rsqrt(jnp.mean(kept * kept, axis=-1, keepdims=True) + EPS)
            hidden[at, head] = (kept * out_gain[:, head]).astype(BF16)
            new.append(sums[h] + rate)
        return tuple(new)

    lax.fori_loop(0, blocks, finish, (jnp.float32(0.0),) * heads)
    for t in range(layers):
        go.arrive(t)

    o_tile = min(128, rows_here)

    def project(start, store):
        @pl.loop(0, rows_here // o_tile)
        def _(i):
            rows = pl.ds(pl.multiple_of(start + i * o_tile, o_tile), o_tile)
            store(pl.ds(pl.multiple_of(i * o_tile, o_tile), o_tile),
                  nt_dot(hidden[rows, :], wo_all[...]).astype(BF16))

    def hand(d):
        return remote(part.at[d - 1], landed.at[d - 1], part_s.at[d - 1], part_r.at[d - 1],
                      (me, (tp + d) % peers))

    for d in range(1, peers):
        def keep(at, value):
            part[d - 1, at, :] = value

        project(((tp + d) % peers) * rows_here, keep)
        hand(d).start()

    def keep_own(at, value):
        own[at, :] = value

    project(base, keep_own)
    for d in range(1, peers):
        hand(d).wait_recv()

    @pl.loop(0, rows_here // tile)
    def _(i):
        at = pl.ds(pl.multiple_of(i * tile, tile), tile)
        total = own[at, :].astype(F32)
        for d in range(1, peers):
            total = total + landed[d - 1, at, :].astype(F32)
        out[at, :] = total.astype(BF16)

    gk.drain()
    gq.drain()
    go.drain()
    for d in range(1, peers):
        send_normed(d).wait_send()
        hand(d).wait_send()
    for h in range(heads):
        pair(0, h, x_dev).wait_send()
        pair(1, h, y_dev).wait_send()

    @pl.when(z < layers - 1)
    def _():
        for h in range(heads):
            remote(z_send.at[h], z_recv.at[h], zs_s.at[h], zs_r.at[h], up_dev).wait_send()


def shards(tokens, norm_gain, w_query, w_key, w_value, decay_rate, state_init, out_gain, w_out):
    n_sp, peers = lax.axis_size("sp"), lax.axis_size("tp")
    layers = n_sp // 4
    rows_here, width = tokens.shape
    span = rows_here * peers
    cols = w_query.shape[1]
    heads = cols // HEAD_DIM
    blocks = span // BLOCK
    half = HEAD_DIM // 2
    freq = ROPE_BASE ** (-jnp.arange(half, dtype=F32) / half)
    freq = jnp.concatenate([freq, freq])[None]
    vmem = pl.BlockSpec(memory_space=pltpu.VMEM)
    hbm = pl.BlockSpec(memory_space=pl.ANY)
    smem = pl.BlockSpec(memory_space=pltpu.SMEM)
    dma = pltpu.SemaphoreType.DMA
    others = max(peers - 1, 1)
    gather_sems = [dma((layers, 3))] * 4 + [dma((layers,))] * 3
    v = pltpu.VMEM
    return pl.pallas_call(
        functools.partial(kernel, layers, peers),
        out_shape=jax.ShapeDtypeStruct((rows_here, width), BF16),
        in_specs=[vmem, vmem, hbm, hbm, hbm, hbm, smem, vmem, vmem, vmem],
        out_specs=vmem,
        scratch_shapes=[
            v((width, 2 * cols), BF16), v((width, cols), BF16), v((width, cols), BF16),
            v((span, width), BF16),
            v((span, 3 * cols), F32), v((span, HEAD_DIM), F32), v((span, HEAD_DIM), F32),
            v((span, cols), BF16), v((span, cols), BF16), v((span, cols), BF16),
            v((span, cols), F32), v((blocks, heads, HEAD_DIM, HEAD_DIM), F32),
            v((heads, HEAD_DIM, HEAD_DIM), F32), v((span, cols), BF16),
            v((others, rows_here, width), BF16), v((others, rows_here, width), BF16),
            v((rows_here, width), BF16),
            v((2, heads, HEAD_DIM + 16, HEAD_DIM), BF16), v((2, heads, HEAD_DIM + 16, HEAD_DIM), BF16),
            v((heads, HEAD_DIM, HEAD_DIM), F32), v((heads, 8, HEAD_DIM), F32),
            v((heads, 8, HEAD_DIM), F32),
            v((heads, HEAD_DIM, HEAD_DIM), BF16), v((heads, HEAD_DIM, HEAD_DIM), BF16),
            v((heads, HEAD_DIM, HEAD_DIM), F32),
            dma((4,)), dma((others,)), dma((others,)), dma((others,)), dma((others,)),
            dma((2, heads)), dma((2, heads)), dma((heads,)), dma((heads,)),
        ] + gather_sems * 3,
        compiler_params=pltpu.CompilerParams(
            collective_id=0, has_side_effects=True, vmem_limit_bytes=62 * 1024 * 1024),
    )(tokens, norm_gain[None], w_query, w_key, w_value, w_out.T, decay_rate, state_init,
      out_gain[None], freq)


def solution(mesh):
    in_specs = (
        P(("sp", "tp"), None),
        P(),
        P("sp", "tp"),
        P("sp", "tp"),
        P("sp", "tp"),
        P("sp", "tp"),
        P("tp", None, None),
        P("tp"),
        P("tp", "sp"),
    )
    out_specs = P(("sp", "tp"), None)
    return jax.shard_map(shards, mesh=mesh, in_specs=in_specs, out_specs=out_specs, check_vma=False)
```

profile of v0, /device:TPU:1, one launch (start us, length us, event | category | flops | bytes accessed | tf_op | source)
XLA Modules:
  0.0 102.4 jit_solution(3285745498919897319)
XLA Ops:
  0.0 0.6 maximum_bitcast_fusion.freq
  0.6 1.3 %copy.11.rates = f32[8,4]{1,0:T(8,128)} copy(f32[8,4]{0,1:T(4,128)} %param.14) | data formatting | bytes 256 | tf_op args[5]
  2.0 1.7 %copy.10 = bf16[512,128]{0,1:T(8,128)(2,1)} copy(bf16[512,128]{1,0:T(8,128)(2,1)} %param.17) | data formatting | bytes 262144 | tf_op args[8]
  3.6 95.6 %shard_map.91 = bf16[512,2048]{1,0:T(8,128)(2,1)} custom-call(bf16[512,2048]{1,0:T(8,128)(2,1)} %tokens.1, f32[1,2048]{1,0:T(1,128)} %bitcast.6, bf16[128,512]{1,0:T(8,128)(2,1)} %wq.1, bf16[128,512]{1,0:T(8,128)(2,1)} %wk.1, bf16[128,512]{1,0:T(8,128)(2,1)} %wv.1, bf16[128,512]{1,0:T(8,128)(2,1)} %bitcast.5, f32[8,4]{1,0:T(8,128)} %copy.11.rates, ...), custom_call_target="tpu_custom_call" | custom-call | tf_op jit(solution)/shard_map/pallas_call | solution.py:462
  99.3 3.2 %copy.13 = bf16[512,2048]{1,0:T(8,128)(2,1)} copy(bf16[512,2048]{1,0:T(8,128)(2,1)} %shard_map.91) | data formatting | bytes 4194304
  (1 shorter events, 0.0 us)
where the time goes:
time: 103 us; the launch traced here: 102 us
  Pallas kernels  95.6 us (93%)
  local copies, waits for them, and re-layouts  6.17 us (6%)
    pallas_call x1, Pallas kernels, shards(): pl.pallas_call(functools.partial(kernel, layers, peers), out_shape=jax.Sh...  95.6 us
    unnamed x3, local copies, waits for them, and re-layouts  6.17 us

commit v1 on v0

v1 whole, which is shorter than its diff:
```python
import functools

import jax
import jax.numpy as jnp
import numpy as np
from jax import lax
from jax.experimental import pallas as pl
from jax.experimental.pallas import tpu as pltpu
from jax.sharding import PartitionSpec as P

HEAD_DIM = 128
BLOCK = 128
EPS = 0.1
ROPE_BASE = 10000.0
MESH = pl.DeviceIdType.MESH
F32 = jnp.float32
BF16 = jnp.bfloat16


def remote(src, dst, send, recv, device):
    return pltpu.make_async_remote_copy(
        src_ref=src, dst_ref=dst, send_sem=send, recv_sem=recv, device_id=device, device_id_type=MESH
    )


class Gather:
    def __init__(self, buf, layers, place, sems):
        self.buf, self.layers, self.place = buf, layers, place
        self.z, self.y, self.x, self.tp = place
        self.rows = buf.shape[0] // (4 * layers)
        self.r_x, self.r_y, self.r_z, self.r_w, self.sent = sems
        self.inner = (self.z > 0) & (self.z < layers - 1)

    def at(self, zi, yi, xi, piece=None):
        start = ((zi * 2 + yi) * 2 + xi) * self.rows
        if piece is None:
            return self.buf.at[pl.ds(pl.multiple_of(start, self.rows), self.rows)]
        half = self.rows // 2
        return self.buf.at[pl.ds(pl.multiple_of(start + piece * half, half), half)]

    def device(self, zi, yi, xi):
        return ((zi * 2 + yi) * 2 + xi, self.tp)

    def layer(self, t):
        zi, bit = self.z, 1
        while bit < self.layers:
            if t & bit:
                zi = zi + bit - 2 * bit * ((self.z // bit) % 2)
            bit *= 2
        return zi

    def copy_x(self, t, j):
        ref = self.at(self.layer(t), 1 - self.y if j == 2 else self.y, self.x, (0, 1, 0, None)[j])
        return remote(ref, ref, self.sent.at[0], self.r_x.at[t // 2, j],
                      self.device(self.z, self.y, 1 - self.x))

    def copy_y(self, t, j):
        ref = self.at(self.layer(t), self.y, 1 - self.x if j == 2 else self.x, (1, 0, 1, None)[j])
        return remote(ref, ref, self.sent.at[0], self.r_y.at[t // 2, j],
                      self.device(self.z, 1 - self.y, self.x))

    def copy_w(self, t, j):
        ref = self.at(self.layer(t), 1 - self.y, 1 - self.x, j)
        return remote(ref, ref, self.sent.at[0], self.r_w.at[t // 2, j],
                      self.device(self.layer(1), self.y, self.x))

    def copy_z(self, zi, step):
        ref = self.at(zi, self.y, self.x)
        return remote(ref, ref, self.sent.at[1], self.r_z.at[zi],
                      self.device(self.z + step, self.y, self.x))

    def order(self, t):
        z, last = self.z, self.layers - 1
        near = z - (t + 1) // 2 if t % 2 else z + t // 2
        m = jnp.minimum(z, last - z)
        far = jnp.where(z < last - z, t, last - t)
        return jnp.where(t <= 2 * m, near, far)

    def along(self, zi, act):
        @pl.when((zi <= self.z) & (self.z < self.layers - 1))
        def _():
            act(self.copy_z(zi, 1))

        @pl.when((zi >= self.z) & (self.z > 0))
        def _():
            act(self.copy_z(zi, -1))

    def lead(self):
        self.along(self.z, lambda copy: copy.start())

    def take(self, t, when=None):
        zi = self.order(t)

        def go():
            self.copy_z(zi, 1).wait_recv()
            self.along(zi, lambda copy: copy.start())

        go() if when is None else pl.when(when)(go)

    def stage(self, s):
        if self.layers != 4:
            if s == 1:
                for t in range(1, self.layers):
                    self.take(t)
            return
        if s == 1:
            self.take(1)
            self.take(2, self.inner)
        elif s == 2:
            self.take(2, jnp.logical_not(self.inner))
            self.take(3, self.inner)
        else:
            self.take(3, jnp.logical_not(self.inner))

    def spread(self, t):
        if t % 2:
            self.copy_x(t, 3).start()
            self.copy_y(t, 3).start()
            return
        self.copy_y(t, 1).start()
        self.copy_x(t, 1).start()
        self.copy_x(t, 0).start()
        self.copy_y(t, 0).start()

    def cross(self, t):
        self.copy_y(t, 1).wait_recv()
        self.copy_x(t, 2).start()
        self.copy_x(t, 1).wait_recv()
        self.copy_y(t, 2).start()

    def swap(self, t):
        self.copy_x(t, 2).wait_recv()
        self.copy_w(t, 0).start()
        self.copy_y(t, 2).wait_recv()
        self.copy_w(t, 1).start()

    def arrive(self, t):
        if t % 2:
            self.copy_x(t, 3).wait_recv()
            self.copy_y(t, 3).wait_recv()
            self.copy_w(t - 1, 0).wait_recv()
            self.copy_w(t - 1, 1).wait_recv()
        else:
            self.copy_x(t, 0).wait_recv()
            self.copy_y(t, 0).wait_recv()
        return self.layer(t)

    def drain(self):
        def sent(k, shards):
            ref = self.buf.at[pl.ds(0, shards * self.rows)]
            remote(ref, ref, self.sent.at[k], self.r_z.at[0], self.device(self.z, self.y, 1 - self.x)).wait_send()

        sent(0, 3 * self.layers)
        pl.when(self.inner)(lambda: sent(1, self.layers + 1))
        pl.when(jnp.logical_not(self.inner))(lambda: sent(1, 1))


def nt_dot(a, b):
    return lax.dot_general(a, b, (((1,), (1,)), ((), ())), preferred_element_type=F32)


def tn_dot(a, b):
    return lax.dot_general(a, b, (((0,), (0,)), ((), ())), preferred_element_type=F32)


SCOPE = jax.named_scope


def kernel(layers, peers, tokens, gain_in, wq, wk, wv, wo, rates_in, state_in, out_gain_in, freq_in, out,
           gain, rates, state_init, out_gain, freq, small_sem, wkv_all, wq_all, wo_all, wo_own, toks, normed, acc, cosine, sine, q_rot, k_rot, v_row, weigh, inner,
           prev, state, hidden, part, landed, tot_send, tot_recv, excl, excl_d, pl_send, pl_recv,
           in_send, in_recv, start, incoming, local_sem, tok_sem, nrm_s, nrm_r, part_s, part_r, t_s, t_r,
           p_s, p_r, i_s, i_r,
           *gather_sems):
    me, tp = lax.axis_index("sp"), lax.axis_index("tp")
    z, y, x = me // 4, (me // 2) % 2, me % 2
    rows_here, width = tokens.shape
    span = rows_here * peers
    cols = wq.shape[1]
    heads = cols // HEAD_DIM
    blocks = span // BLOCK
    shard = wq.shape[0]
    place = (z, y, x, tp)
    gk = Gather(wkv_all, layers, place, gather_sems[:5])
    gq = Gather(wq_all, layers, place, gather_sems[5:10])
    go = Gather(wo_all, layers, place, gather_sems[10:])
    parts = nrm_s.shape[1]
    chunk = rows_here // parts

    mine = pl.ds(pl.multiple_of(me * shard, shard), shard)
    fills = [
        pltpu.make_async_copy(src, dst, local_sem.at[i])
        for i, (src, dst) in enumerate((
            (wk, wkv_all.at[mine, pl.ds(0, cols)]),
            (wv, wkv_all.at[mine, pl.ds(cols, cols)]),
            (wq, wq_all.at[mine]),
            (wo, wo_own),
        ))
    ]
    loads = [
        pltpu.make_async_copy(tokens.at[pl.ds(c * chunk, chunk)], toks.at[pl.ds(c * chunk, chunk)],
                              tok_sem.at[c])
        for c in range(parts)
    ]
    smalls = [
        pltpu.make_async_copy(src, dst, small_sem.at[i])
        for i, (src, dst) in enumerate((
            (gain_in, gain), (freq_in, freq), (rates_in, rates), (out_gain_in, out_gain),
            (state_in, state_init)))
    ]
    barrier = pltpu.get_barrier_semaphore()

    def greet(device):
        pl.semaphore_signal(barrier, inc=1, device_id=device, device_id_type=MESH)

    greet(gq.device(z, y, 1 - x))
    greet(gq.device(z, 1 - y, x))
    greet(gq.device(z, 1 - y, 1 - x))
    for d in range(1, peers):
        greet((me, (tp + d) % peers))
    for k in range(1, layers):
        pl.when(z + k < layers)(lambda: greet(gq.device(z + k, y, x)))
        pl.when(z >= k)(lambda: greet(gq.device(z - k, y, x)))

    for copy in fills + loads + smalls:
        copy.start()

    out_shard = wo.shape[1]
    for fill in fills[:3]:
        fill.wait()
    with SCOPE("barrier"):
        pl.semaphore_wait(barrier, 1 + peers + layers)

    gk.lead()
    gk.spread(0)
    gq.lead()

    base = pl.multiple_of(tp * rows_here, rows_here)
    tile = min(64, chunk)

    def send_normed(d, c):
        ref = normed.at[pl.ds(pl.multiple_of(base + c * chunk, chunk), chunk)]
        return remote(ref, ref, nrm_s.at[d - 1, c], nrm_r.at[d - 1, c], (me, (tp + d) % peers))

    for copy in smalls:
        copy.wait()
    for c in range(parts):
        loads[c].wait()

        @pl.loop(c * chunk // tile, (c + 1) * chunk // tile)
        def _(i):
            at = pl.ds(pl.multiple_of(i * tile, tile), tile)
            u = toks[at, :].astype(F32)
            scale = lax.rsqrt(jnp.mean(u * u, axis=-1, keepdims=True) + EPS)
            normed[pl.ds(pl.multiple_of(base + i * tile, tile), tile), :] = (
                u * scale * gain[...]
            ).astype(BF16)

        for d in range(1, peers):
            send_normed(d, c).start()

    fills[3].wait()
    wo_all[pl.ds(pl.multiple_of(me * out_shard, out_shard), out_shard), :] = wo_own[...].T

    def trig(i, carry):
        at = pl.ds(pl.multiple_of(i * BLOCK, BLOCK), BLOCK)
        pos = lax.broadcasted_iota(jnp.int32, (BLOCK, HEAD_DIM), 0) + (me * span + i * BLOCK)
        angle = pos.astype(F32) * freq[...]
        lane = lax.broadcasted_iota(jnp.int32, (BLOCK, HEAD_DIM), 1)
        sin = jnp.sin(angle)
        cosine[at, :] = jnp.cos(angle)
        sine[at, :] = jnp.where(lane < HEAD_DIM // 2, -sin, sin)
        return carry

    deep = 4 * shard
    m_tile = min(256, span)

    def product(gather, t, n, first, count):
        with SCOPE("arrive"):
            for i in range(n):
                zi = gather.arrive(t + i)
        at_k = pl.ds(pl.multiple_of((zi // n) * (n * deep), n * deep), n * deep)
        with SCOPE("product"):
            @pl.loop(0, span // m_tile)
            def _(i):
                at = pl.ds(pl.multiple_of(i * m_tile, m_tile), m_tile)
                for c in range(count):
                    term = jnp.dot(normed[at, at_k], gather.buf[at_k, c * cols:(c + 1) * cols],
                                   preferred_element_type=F32)
                    at_c = pl.ds((first + c) * cols, cols)
                    acc[at, at_c] = term if t == 0 else acc[at, at_c] + term

    gap = (lax.broadcasted_iota(jnp.int32, (BLOCK, BLOCK), 0)
           - lax.broadcasted_iota(jnp.int32, (BLOCK, BLOCK), 1)).astype(F32)
    row = lax.broadcasted_iota(jnp.int32, (BLOCK, HEAD_DIM), 0).astype(F32)

    def states(b, sums):
        at = pl.ds(pl.multiple_of(b * BLOCK, BLOCK), BLOCK)
        cos, sin = cosine[at, :], sine[at, :]
        new = []
        for h in range(heads):
            rate = rates[h, b]
            head = pl.ds(h * HEAD_DIM, HEAD_DIM)
            u = acc[at, pl.ds(cols + h * HEAD_DIM, HEAD_DIM)]
            k = (u * cos + pltpu.roll(u, HEAD_DIM // 2, 1) * sin).astype(BF16)
            v = acc[at, pl.ds(2 * cols + h * HEAD_DIM, HEAD_DIM)].astype(BF16)
            k_rot[at, head] = k
            v_row[at, head] = v
            tail = jnp.exp(-(BLOCK - 1.0 - row) * rate) * HEAD_DIM ** (-0.5)
            kv = tn_dot((k.astype(F32) * tail).astype(BF16), v)
            now = state[h]
            prev[b, h] = now
            state[h] = jnp.exp(jnp.full((1, HEAD_DIM), -float(BLOCK), F32) * rate) * now + kv
            new.append(sums[h] + rate)
        return tuple(new)

    def decay_of(total):
        return jnp.exp(jnp.full((1, HEAD_DIM), -float(BLOCK), F32) * total)

    corner = 2 * y + x
    slots = max(heads // 4, 1)
    owner = None if heads >= 4 else corner < heads

    def toward(r):
        return (y + r // 2 - 2 * y * (r // 2)) * 2 + (x + r % 2 - 2 * x * (r % 2))

    def guard(r, act):
        act() if heads >= 4 else pl.when(toward(r) < heads)(act)

    def beside(r):
        return (4 * z + toward(r), tp)

    def total_to(r, i):
        return remote(tot_send.at[4 * i + toward(r)], tot_recv.at[i, r], t_s.at[i, r], t_r.at[i, r], beside(r))

    def plane_to(k, i):
        return remote(pl_send.at[i], pl_recv.at[i, z], p_s.at[i, k], p_r.at[i, z], (4 * (z + k) + corner, tp))

    def plane_from(zz, i):
        return remote(pl_send.at[i], pl_recv.at[i, zz], p_s.at[i, 0], p_r.at[i, zz], (4 * z + corner, tp))

    def start_to(r, i):
        return remote(in_send.at[i, r], in_recv.at[i, r], i_s.at[i, r], i_r.at[i, r], beside(r))

    def packed(decay, value):
        return jnp.concatenate([value, jnp.broadcast_to(decay, (16, HEAD_DIM))], axis=0).astype(BF16)

    def opened(ref):
        return ref[HEAD_DIM:, :].astype(F32)[:1], ref[:HEAD_DIM, :].astype(F32)

    def mine_only(act):
        act() if heads >= 4 else pl.when(owner)(act)

    def send_totals():
        for h in range(heads):
            tot_send[h] = packed(decay_of(sums[h]), state[h])
        for r in (3, 1, 2):
            def go_out():
                for i in range(slots):
                    total_to(r, i).start()
            guard(r, go_out)

    def plane_totals():
        def act():
            for i in range(slots):
                tot_recv[i, 0] = tot_send[4 * i + corner]
                for r in (1, 2, 3):
                    total_to(r, i).wait_recv()
                decay, value = jnp.ones((1, HEAD_DIM), F32), jnp.zeros((HEAD_DIM, HEAD_DIM), F32)
                for j in range(4):
                    excl[i, j], excl_d[i, j] = value, jnp.broadcast_to(decay, (8, HEAD_DIM))
                    d, v = opened(tot_recv.at[i, toward(j)])
                    decay, value = decay * d, value * d + v
                pl_send[i] = packed(decay, value)
                for k in range(1, layers):
                    @pl.when(z + k < layers)
                    def _():
                        plane_to(k, i).start()
        mine_only(act)

    def starts():
        def act():
            for i in range(slots):
                start[...] = state_init[4 * i + corner]
                for zz in range(layers - 1):
                    @pl.when(zz < z)
                    def _():
                        plane_from(zz, i).wait_recv()
                        d, v = opened(pl_recv.at[i, zz])
                        start[...] = start[...] * d + v
                for r in (3, 1, 2):
                    at = toward(r)
                    in_send[i, r] = (excl_d[i, at][:1] * start[...] + excl[i, at]).astype(BF16)
                    start_to(r, i).start()
                incoming[4 * i + corner] = excl_d[i, corner][:1] * start[...] + excl[i, corner]
        mine_only(act)

    def started():
        for i in range(slots):
            for r in (1, 2, 3):
                def act():
                    start_to(r, i).wait_recv()
                    incoming[4 * i + toward(r)] = in_recv[i, r].astype(F32)
                guard(r, act)

    def sent_states():
        for i in range(slots):
            for r in (1, 2, 3):
                guard(r, total_to(r, i).wait_send)

            def act():
                for r in (1, 2, 3):
                    start_to(r, i).wait_send()
                for k in range(1, layers):
                    pl.when(z + k < layers)(plane_to(k, i).wait_send)
            mine_only(act)

    def turn(b, carry):
        at = pl.ds(pl.multiple_of(b * BLOCK, BLOCK), BLOCK)
        cos, sin = cosine[at, :], sine[at, :]
        for h in range(heads):
            head = pl.ds(h * HEAD_DIM, HEAD_DIM)
            u = acc[at, head]
            q_rot[at, head] = (u * cos + pltpu.roll(u, HEAD_DIM // 2, 1) * sin).astype(BF16)
        return carry

    def scores(b):
        at = pl.ds(pl.multiple_of(b * BLOCK, BLOCK), BLOCK)
        for h in range(heads):
            head = pl.ds(h * HEAD_DIM, HEAD_DIM)
            fall = jnp.where(gap >= 0.0, jnp.exp(-jnp.maximum(gap, 0.0) * rates[h, b]), 0.0)
            score = nt_dot(q_rot[at, head], k_rot[at, head]) * (fall * HEAD_DIM ** (-0.5))
            weigh[at, head] = score.astype(BF16)

    def gathered(b):
        at = pl.ds(pl.multiple_of(b * BLOCK, BLOCK), BLOCK)
        for h in range(heads):
            head = pl.ds(h * HEAD_DIM, HEAD_DIM)
            inner[at, head] = jnp.dot(weigh[at, head], v_row[at, head], preferred_element_type=F32)

    def inside(b, carry):
        gathered(b - 1)
        scores(b)
        return carry

    def finish(b, sums):
        at = pl.ds(pl.multiple_of(b * BLOCK, BLOCK), BLOCK)
        new = []
        for h in range(heads):
            rate = rates[h, b]
            head = pl.ds(h * HEAD_DIM, HEAD_DIM)
            before = prev[b, h] + decay_of(sums[h]) * incoming[h]
            read = jnp.exp(-(row + 1.0) * rate)
            kept = inner[at, head] + read * jnp.dot(
                q_rot[at, head], before.astype(BF16), preferred_element_type=F32)
            kept = kept * lax.rsqrt(jnp.mean(kept * kept, axis=-1, keepdims=True) + EPS)
            hidden[at, head] = (kept * out_gain[:, head]).astype(BF16)
            new.append(sums[h] + rate)
        return tuple(new)

    wide = 4 * out_shard
    o_tile = min(512, rows_here)

    def hand(d, t):
        return remote(part.at[d - 1, t], landed.at[d - 1, t], part_s.at[d - 1, t], part_r.at[d - 1, t],
                      (me, (tp + d) % peers))

    def pieces(t):
        with SCOPE("oarrive"):
            zi = go.arrive(t)
        return pl.ds(pl.multiple_of(zi * wide, wide), wide)

    def theirs(t):
        rows_o = pieces(t)
        with SCOPE("theirs"):
            for d in range(1, peers):
                @pl.loop(0, rows_here // o_tile)
                def _(i):
                    start = ((tp + d) % peers) * rows_here
                    rows = pl.ds(pl.multiple_of(start + i * o_tile, o_tile), o_tile)
                    part[d - 1, t, pl.ds(pl.multiple_of(i * o_tile, o_tile), o_tile), :] = nt_dot(
                        hidden[rows, :], wo_all[rows_o, :]).astype(BF16)

                hand(d, t).start()

    def ours(t):
        at_c = pl.ds(pl.multiple_of(go.layer(t) * wide, wide), wide)
        with SCOPE("w_hand"):
            for d in range(1, peers):
                hand(d, t).wait_recv()
        with SCOPE("ours"):
            @pl.loop(0, rows_here // o_tile)
            def _(i):
                at = pl.ds(pl.multiple_of(i * o_tile, o_tile), o_tile)
                rows = pl.ds(pl.multiple_of(base + i * o_tile, o_tile), o_tile)
                value = nt_dot(hidden[rows, :], wo_all[at_c, :])
                for d in range(1, peers):
                    value = value + landed[d - 1, t, at, :].astype(F32)
                out[at, at_c] = value.astype(BF16)

    def sc(name, fn, *args):
        with SCOPE(name):
            fn(*args)

    early = range(1, layers - 2 if layers > 4 else 2)
    evens = range(2, layers, 2)
    sc("kcross0", gk.cross, 0)
    sc("trig", lambda: lax.fori_loop(0, blocks // 2, trig, 0))
    sc("kstage1", gk.stage, 1)
    for t in early:
        gk.spread(t)
    gq.spread(0)
    sc("trig", lambda: lax.fori_loop(blocks // 2, blocks, trig, 0))
    with SCOPE("nrmwait"):
        for d in range(1, peers):
            for c in range(parts):
                send_normed(d, c).wait_recv()
    sc("qstage1", gq.stage, 1)
    if layers > 2:
        sc("kstage2", gk.stage, 2)
        gk.spread(layers - 2)
    sc("kswap0", gk.swap, 0)
    for t in evens:
        sc("kcross2", gk.cross, t)
    if layers > 2:
        sc("kstage3", gk.stage, 3)
        gk.spread(layers - 1)
    for t in evens:
        sc("kswap2", gk.swap, t)
    if layers > 2:
        sc("qstage2", gq.stage, 2)
        gq.spread(layers - 2)
    sc("qcross0", gq.cross, 0)
    for t in early:
        gq.spread(t)
    product(gk, 0, 2, 1, 2)
    for t in evens:
        product(gk, t, 1, 1, 2)
        product(gk, t + 1, 1, 1, 2)

    for h in range(heads):
        state[h] = jnp.zeros((HEAD_DIM, HEAD_DIM), F32)
    with SCOPE("states"):
        sums = lax.fori_loop(0, blocks, states, (jnp.float32(0.0),) * heads)
    sc("send_tot", send_totals)
    for t in evens:
        sc("qcross2", gq.cross, t)
    go.lead()
    sc("qswap0", gq.swap, 0)
    if layers > 2:
        sc("qstage3", gq.stage, 3)
        gq.spread(layers - 1)
    go.spread(0)
    sc("plane_tot", plane_totals)
    for t in evens:
        sc("qswap2", gq.swap, t)
    sc("ostage1", go.stage, 1)
    product(gq, 0, 2, 0, 1)
    sc("ocross0", go.cross, 0)
    if layers > 2:
        sc("ostage2", go.stage, 2)
        go.spread(layers - 2)
    for t in early:
        go.spread(t)
    sc("starts", starts)
    for t in evens:
        product(gq, t, 2, 0, 1)
    cut = [max(1, blocks * i // 4) for i in range(5)]
    with SCOPE("turn"):
        lax.fori_loop(0, blocks, turn, 0)
    scores(0)
    sc("oswap0", go.swap, 0)
    with SCOPE("inside"):
        lax.fori_loop(1, cut[2], inside, 0)
    if layers > 2:
        sc("ostage3", go.stage, 3)
    for t in evens:
        sc("ocross2", go.cross, t)
    if layers > 2:
        go.spread(layers - 1)
    with SCOPE("inside"):
        lax.fori_loop(cut[2], blocks, inside, 0)
        gathered(blocks - 1)
    sc("started", started)
    with SCOPE("finish"):
        lax.fori_loop(0, blocks, finish, (jnp.float32(0.0),) * heads)
    for t in evens:
        sc("oswap2", go.swap, t)
    for t in range(layers + 2):
        if t < layers:
            theirs(t)
        if t >= 2:
            ours(t - 2)

    with SCOPE("drain"):
        gk.drain()
        gq.drain()
        go.drain()
        for d in range(1, peers):
            for c in range(parts):
                send_normed(d, c).wait_send()
            for t in range(layers):
                hand(d, t).wait_send()
        sent_states()


def shards(tokens, norm_gain, w_query, w_key, w_value, decay_rate, state_init, out_gain, w_out):
    n_sp, peers = lax.axis_size("sp"), lax.axis_size("tp")
    layers = n_sp // 4
    rows_here, width = tokens.shape
    span = rows_here * peers
    cols = w_query.shape[1]
    heads = cols // HEAD_DIM
    blocks = span // BLOCK
    half = HEAD_DIM // 2
    wide = 4 * w_out.shape[1]
    freq = ROPE_BASE ** (-np.arange(half, dtype=np.float64) / half)
    freq = np.concatenate([freq, freq])[None].astype(np.float32)
    vmem = pl.BlockSpec(memory_space=pltpu.VMEM)
    hbm = pl.BlockSpec(memory_space=pl.ANY)
    dma = pltpu.SemaphoreType.DMA
    others, slots = max(peers - 1, 1), max(heads // 4, 1)
    parts = 2
    gather_sems = [dma((layers // 2, 4))] * 2 + [dma((layers,)), dma((layers // 2, 2)), dma((2,))]
    v = pltpu.VMEM
    return pl.pallas_call(
        functools.partial(kernel, layers, peers),
        out_shape=jax.ShapeDtypeStruct((rows_here, width), BF16),
        in_specs=[hbm] * 10,
        out_specs=vmem,
        scratch_shapes=[
            v((1, width), F32), pltpu.SMEM((heads, blocks), F32), v((heads, HEAD_DIM, HEAD_DIM), F32),
            v((1, cols), F32), v((1, HEAD_DIM), F32), dma((5,)),
            v((width, 2 * cols), BF16), v((width, cols), BF16), v((width, cols), BF16),
            v(w_out.shape, BF16), v((rows_here, width), BF16),
            v((span, width), BF16),
            v((span, 3 * cols), F32), v((span, HEAD_DIM), F32), v((span, HEAD_DIM), F32),
            v((span, cols), BF16), v((span, cols), BF16), v((span, cols), BF16), v((span, cols), BF16),
            v((span, cols), F32), v((blocks, heads, HEAD_DIM, HEAD_DIM), F32),
            v((heads, HEAD_DIM, HEAD_DIM), F32), v((span, cols), BF16),
            v((others, layers, rows_here, wide), BF16), v((others, layers, rows_here, wide), BF16),
            v((heads, HEAD_DIM + 16, HEAD_DIM), BF16), v((slots, 4, HEAD_DIM + 16, HEAD_DIM), BF16),
            v((slots, 4, HEAD_DIM, HEAD_DIM), F32), v((slots, 4, 8, HEAD_DIM), F32),
            v((slots, HEAD_DIM + 16, HEAD_DIM), BF16), v((slots, layers, HEAD_DIM + 16, HEAD_DIM), BF16),
            v((slots, 4, HEAD_DIM, HEAD_DIM), BF16), v((slots, 4, HEAD_DIM, HEAD_DIM), BF16),
            v((HEAD_DIM, HEAD_DIM), F32), v((heads, HEAD_DIM, HEAD_DIM), F32),
            dma((4,)), dma((parts,)), dma((others, parts)), dma((others, parts)),
            dma((others, layers)), dma((others, layers)),
            dma((slots, 4)), dma((slots, 4)), dma((slots, layers)), dma((slots, layers)),
            dma((slots, 4)), dma((slots, 4)),
        ] + gather_sems * 3,
        compiler_params=pltpu.CompilerParams(
            collective_id=0, has_side_effects=True, vmem_limit_bytes=46 * 1024 * 1024),
    )(*(pltpu.with_memory_space_constraint(u, pltpu.HBM) for u in (
        tokens, norm_gain[None], w_query, w_key, w_value, w_out, decay_rate.T, state_init,
        out_gain[None], jnp.asarray(freq))))


def solution(mesh):
    in_specs = (
        P(("sp", "tp"), None),
        P(),
        P("sp", "tp"),
        P("sp", "tp"),
        P("sp", "tp"),
        P("sp", "tp"),
        P("tp", None, None),
        P("tp"),
        P("tp", "sp"),
    )
    out_specs = P(("sp", "tp"), None)
    return jax.shard_map(shards, mesh=mesh, in_specs=in_specs, out_specs=out_specs, check_vma=False)
```

time: 103 us -> 76.4 us (0.74)
  Pallas kernels: 95.6 us -> 74.9 us
  local copies, waits for them, and re-layouts: 6.17 us -> 1.32 us
    pallas_call x1, Pallas kernels: 95.6 us -> 74.9 us  [shards(): pl.pallas_call(functools.partial(kernel, layers, peers), out_shape=jax.Sh...]
    unnamed x3 -> x1, local copies, waits for them, and re-layouts: 6.17 us -> 1.32 us
where the time goes in v1:
time: 76.4 us; the launch traced here: 76.2 us
  Pallas kernels  74.9 us (98%)
  local copies, waits for them, and re-layouts  1.32 us (2%)
    pallas_call x1, Pallas kernels, shards(): pl.pallas_call(functools.partial(kernel, layers, peers), out_shape=jax.Sh...  74.9 us

profile of v1, /device:TPU:1, one launch (start us, length us, event | category | flops | bytes accessed | tf_op | source)
XLA Modules:
  0.0 76.2 jit_solution(1907943928367643149)
XLA Ops:
  0.0 74.9 %shard_map.100 = bf16[512,2048]{1,0:T(8,128)(2,1)S(1)} custom-call(bf16[512,2048]{1,0:T(8,128)(2,1)} %tokens.1, f32[1,2048]{1,0:T(1,128)} %bitcast.3, bf16[128,512]{1,0:T(8,128)(2,1)} %wq.1, bf16[128,512]{1,0:T(8,128)(2,1)} %wk.1, bf16[128,512]{1,0:T(8,128)(2,1)} %wv.1, bf16[512,128]{1,0:T(8,128)(2,1)} %wo.1, f32[4,8]{1,0:T(4,128)} %bitcast.4, ...), custom_call_target="tpu_custom_call" | custom-call | tf_op jit(solution)/shard_map/pallas_call | solution.py:626
  74.9 1.3 %copy.12 = bf16[512,2048]{1,0:T(8,128)(2,1)} copy(bf16[512,2048]{1,0:T(8,128)(2,1)S(1)} %shard_map.100) | data formatting | bytes 4194304

commit v2 on v1

--- a/solution.py
+++ b/solution.py
@@ -24,8 +24,9 @@
 
 
 class Gather:
-    def __init__(self, buf, layers, place, sems):
+    def __init__(self, buf, layers, place, sems, split=False):
         self.buf, self.layers, self.place = buf, layers, place
+        self.pieces = (0, 1) if split else (None,)
         self.z, self.y, self.x, self.tp = place
         self.rows = buf.shape[0] // (4 * layers)
         self.r_x, self.r_y, self.r_z, self.r_w, self.sent = sems
@@ -64,9 +65,9 @@
         return remote(ref, ref, self.sent.at[0], self.r_w.at[t // 2, j],
                       self.device(self.layer(1), self.y, self.x))
 
-    def copy_z(self, zi, step):
-        ref = self.at(zi, self.y, self.x)
-        return remote(ref, ref, self.sent.at[1], self.r_z.at[zi],
+    def copy_z(self, zi, step, piece):
+        ref = self.at(zi, self.y, self.x, piece)
+        return remote(ref, ref, self.sent.at[1], self.r_z.at[zi, piece or 0],
                       self.device(self.z + step, self.y, self.x))
 
     def order(self, t):
@@ -76,41 +77,66 @@
         far = jnp.where(z < last - z, t, last - t)
         return jnp.where(t <= 2 * m, near, far)
 
-    def along(self, zi, act):
+    def along(self, zi, piece):
         @pl.when((zi <= self.z) & (self.z < self.layers - 1))
         def _():
-            act(self.copy_z(zi, 1))
+            self.copy_z(zi, 1, piece).start()
 
         @pl.when((zi >= self.z) & (self.z > 0))
         def _():
-            act(self.copy_z(zi, -1))
-
-    def lead(self):
-        self.along(self.z, lambda copy: copy.start())
-
-    def take(self, t, when=None):
+            self.copy_z(zi, -1, piece).start()
+
+    def lead(self, late=None):
+        for piece in self.pieces:
+            if late is None or self.layers != 4:
+                if not late:
+                    self.along(self.z, piece)
+                continue
+            even, outer = self.z % 2 == 0, jnp.logical_not(self.inner)
+            odd = jnp.logical_not(even)
+            up = self.inner & even if late else (self.z < self.layers - 1) & (outer | odd)
+            down = self.inner & odd if late else (self.z > 0) & (outer | even)
+            pl.when(up)(lambda: self.copy_z(self.z, 1, piece).start())
+            pl.when(down)(lambda: self.copy_z(self.z, -1, piece).start())
+
+    def take(self, t, pieces, when=None):
         zi = self.order(t)
 
         def go():
-            self.copy_z(zi, 1).wait_recv()
-            self.along(zi, lambda copy: copy.start())
+            for piece in pieces:
+                self.copy_z(zi, 1, piece).wait_recv()
+                self.along(zi, piece)
 
         go() if when is None else pl.when(when)(go)
 
-    def stage(self, s):
+    def stage(self, s, pieces=None):
+        pieces = pieces or self.pieces
         if self.layers != 4:
             if s == 1:
                 for t in range(1, self.layers):
-                    self.take(t)
+                    self.take(t, pieces)
             return
         if s == 1:
-            self.take(1)
-            self.take(2, self.inner)
+            self.take(1, pieces)
+            self.take(2, pieces, self.inner)
         elif s == 2:
-            self.take(2, jnp.logical_not(self.inner))
-            self.take(3, self.inner)
+            self.take(2, pieces, jnp.logical_not(self.inner))
+            self.take(3, pieces, self.inner)
         else:
-            self.take(3, jnp.logical_not(self.inner))
+            self.take(3, pieces, jnp.logical_not(self.inner))
+
+    def middle(self, *order):
+        if self.layers == 4:
+            for t in order:
+                self.take(t, self.pieces, self.inner)
+        elif 1 in order:
+            for t in range(1, self.layers):
+                self.take(t, self.pieces)
+
+    def outer(self, *order):
+        if self.layers == 4:
+            for t in order:
+                self.take(t, self.pieces, jnp.logical_not(self.inner))
 
     def spread(self, t):
         if t % 2:
@@ -148,7 +174,7 @@
     def drain(self):
         def sent(k, shards):
             ref = self.buf.at[pl.ds(0, shards * self.rows)]
-            remote(ref, ref, self.sent.at[k], self.r_z.at[0], self.device(self.z, self.y, 1 - self.x)).wait_send()
+            remote(ref, ref, self.sent.at[k], self.r_z.at[0, 0], self.device(self.z, self.y, 1 - self.x)).wait_send()
 
         sent(0, 3 * self.layers)
         pl.when(self.inner)(lambda: sent(1, self.layers + 1))
@@ -181,7 +207,7 @@
     blocks = span // BLOCK
     shard = wq.shape[0]
     place = (z, y, x, tp)
-    gk = Gather(wkv_all, layers, place, gather_sems[:5])
+    gk = Gather(wkv_all, layers, place, gather_sems[:5], True)
     gq = Gather(wq_all, layers, place, gather_sems[5:10])
     go = Gather(wo_all, layers, place, gather_sems[10:])
     parts = nrm_s.shape[1]
@@ -215,12 +241,10 @@
 
     greet(gq.device(z, y, 1 - x))
     greet(gq.device(z, 1 - y, x))
-    greet(gq.device(z, 1 - y, 1 - x))
     for d in range(1, peers):
         greet((me, (tp + d) % peers))
-    for k in range(1, layers):
-        pl.when(z + k < layers)(lambda: greet(gq.device(z + k, y, x)))
-        pl.when(z >= k)(lambda: greet(gq.device(z - k, y, x)))
+    pl.when(z > 0)(lambda: greet(gq.device(z - 1, y, x)))
+    pl.when(z < layers - 1)(lambda: greet(gq.device(z + 1, y, x)))
 
     for copy in fills + loads + smalls:
         copy.start()
@@ -229,11 +253,11 @@
     for fill in fills[:3]:
         fill.wait()
     with SCOPE("barrier"):
-        pl.semaphore_wait(barrier, 1 + peers + layers)
+        pl.semaphore_wait(
+            barrier, 1 + peers + jnp.minimum(z, 1) + jnp.minimum(layers - 1 - z, 1))
 
     gk.lead()
     gk.spread(0)
-    gq.lead()
 
     base = pl.multiple_of(tp * rows_here, rows_here)
     tile = min(64, chunk)
@@ -502,95 +526,99 @@
         with SCOPE(name):
             fn(*args)
 
-    early = range(1, layers - 2 if layers > 4 else 2)
-    evens = range(2, layers, 2)
+    evens, odds, last = range(2, layers, 2), range(1, layers - 2, 2), layers - 1
+    cut = max(1, blocks // 2)
+
+    def each(name, ts, fn):
+        for t in ts:
+            sc(name, fn, t)
+
     sc("kcross0", gk.cross, 0)
-    sc("trig", lambda: lax.fori_loop(0, blocks // 2, trig, 0))
-    sc("kstage1", gk.stage, 1)
-    for t in early:
-        gk.spread(t)
-    gq.spread(0)
-    sc("trig", lambda: lax.fori_loop(blocks // 2, blocks, trig, 0))
+    sc("kstage1a", gk.stage, 1, (0,))
+    sc("trig", lambda: lax.fori_loop(0, cut, trig, 0))
+    sc("kstage1b", gk.stage, 1, (1,))
+    each("kspread", odds, gk.spread)
+    sc("trig", lambda: lax.fori_loop(cut, blocks, trig, 0))
     with SCOPE("nrmwait"):
         for d in range(1, peers):
             for c in range(parts):
                 send_normed(d, c).wait_recv()
-    sc("qstage1", gq.stage, 1)
-    if layers > 2:
-        sc("kstage2", gk.stage, 2)
-        gk.spread(layers - 2)
+    sc("kstage2a", gk.stage, 2, (0,))
+    sc("kstage2b", gk.stage, 2, (1,))
+    each("kspread", evens, gk.spread)
     sc("kswap0", gk.swap, 0)
-    for t in evens:
-        sc("kcross2", gk.cross, t)
-    if layers > 2:
-        sc("kstage3", gk.stage, 3)
-        gk.spread(layers - 1)
-    for t in evens:
-        sc("kswap2", gk.swap, t)
-    if layers > 2:
-        sc("qstage2", gq.stage, 2)
-        gq.spread(layers - 2)
-    sc("qcross0", gq.cross, 0)
-    for t in early:
-        gq.spread(t)
-    product(gk, 0, 2, 1, 2)
+    gq.lead(False)
+    product(gk, 0, 1, 1, 2)
+    each("kcross2", evens, gk.cross)
+    gq.spread(0)
+    sc("kstage3", gk.stage, 3)
+    gk.spread(last)
+    sc("qmiddle", gq.middle, 1, 2)
+    each("kswap2", evens, gk.swap)
     for t in evens:
         product(gk, t, 1, 1, 2)
-        product(gk, t + 1, 1, 1, 2)
+    sc("qmiddle3", gq.middle, 3)
+    sc("qouter2", gq.outer, 2)
+    gq.lead(True)
+    each("qspread", evens, gq.spread)
+    for t in odds:
+        product(gk, t, 1, 1, 2)
+    sc("qcross0", gq.cross, 0)
+    go.lead(False)
+    product(gk, last, 1, 1, 2)
 
     for h in range(heads):
         state[h] = jnp.zeros((HEAD_DIM, HEAD_DIM), F32)
     with SCOPE("states"):
-        sums = lax.fori_loop(0, blocks, states, (jnp.float32(0.0),) * heads)
+        sums = lax.fori_loop(0, cut, states, (jnp.float32(0.0),) * heads)
+    each("qcross2", evens, gq.cross)
+    sc("omiddle", go.middle, 1, 2)
+    with SCOPE("states"):
+        sums = lax.fori_loop(cut, blocks, states, sums)
     sc("send_tot", send_totals)
-    for t in evens:
-        sc("qcross2", gq.cross, t)
-    go.lead()
     sc("qswap0", gq.swap, 0)
-    if layers > 2:
-        sc("qstage3", gq.stage, 3)
-        gq.spread(layers - 1)
+    sc("qouter3", gq.outer, 3)
+    sc("qouter1", gq.outer, 1)
+    each("qspread", odds, gq.spread)
+    gq.spread(last)
+    each("qswap2", evens, gq.swap)
+    sc("plane_tot", plane_totals)
+    sc("omiddle3", go.middle, 3)
+    go.lead(True)
     go.spread(0)
-    sc("plane_tot", plane_totals)
-    for t in evens:
-        sc("qswap2", gq.swap, t)
-    sc("ostage1", go.stage, 1)
     product(gq, 0, 2, 0, 1)
-    sc("ocross0", go.cross, 0)
-    if layers > 2:
-        sc("ostage2", go.stage, 2)
-        go.spread(layers - 2)
-    for t in early:
-        go.spread(t)
+    sc("oouter2", go.outer, 2)
+    each("ospread", evens, go.spread)
     sc("starts", starts)
     for t in evens:
         product(gq, t, 2, 0, 1)
-    cut = [max(1, blocks * i // 4) for i in range(5)]
+    sc("ocross0", go.cross, 0)
     with SCOPE("turn"):
         lax.fori_loop(0, blocks, turn, 0)
     scores(0)
+    sc("oouter3", go.outer, 3)
+    go.spread(last)
+    each("ocross2", evens, go.cross)
+    with SCOPE("inside"):
+        lax.fori_loop(1, cut, inside, 0)
+    sc("oouter1", go.outer, 1)
+    each("ospread", odds, go.spread)
     sc("oswap0", go.swap, 0)
     with SCOPE("inside"):
-        lax.fori_loop(1, cut[2], inside, 0)
-    if layers > 2:
-        sc("ostage3", go.stage, 3)
-    for t in evens:
-        sc("ocross2", go.cross, t)
-    if layers > 2:
-        go.spread(layers - 1)
-    with SCOPE("inside"):
-        lax.fori_loop(cut[2], blocks, inside, 0)
+        lax.fori_loop(cut, blocks, inside, 0)
         gathered(blocks - 1)
     sc("started", started)
     with SCOPE("finish"):
-        lax.fori_loop(0, blocks, finish, (jnp.float32(0.0),) * heads)
-    for t in evens:
-        sc("oswap2", go.swap, t)
-    for t in range(layers + 2):
-        if t < layers:
-            theirs(t)
-        if t >= 2:
-            ours(t - 2)
+        sums = lax.fori_loop(0, cut, finish, (jnp.float32(0.0),) * heads)
+    each("oswap2", evens, go.swap)
+    with SCOPE("finish"):
+        lax.fori_loop(cut, blocks, finish, sums)
+    turns = (0,) + tuple(evens) + tuple(odds) + (last,) if layers > 2 else (0, 1)
+    for i in range(layers + 2):
+        if i < layers:
+            theirs(turns[i])
+        if i >= 2:
+            ours(turns[i - 2])
 
     with SCOPE("drain"):
         gk.drain()
@@ -621,7 +649,7 @@
     dma = pltpu.SemaphoreType.DMA
     others, slots = max(peers - 1, 1), max(heads // 4, 1)
     parts = 2
-    gather_sems = [dma((layers // 2, 4))] * 2 + [dma((layers,)), dma((layers // 2, 2)), dma((2,))]
+    gather_sems = [dma((layers // 2, 4))] * 2 + [dma((layers, 2)), dma((layers // 2, 2)), dma((2,))]
     v = pltpu.VMEM
     return pl.pallas_call(
         functools.partial(kernel, layers, peers),

time: 76.4 us -> 73.1 us (0.957)
  Pallas kernels: 74.9 us -> 71.4 us
    pallas_call x1, Pallas kernels: 74.9 us -> 71.4 us  [shards(): pl.pallas_call(functools.partial(kernel, layers, peers), out_shape=jax.Sh...]
where the time goes in v2:
time: 73.1 us; the launch traced here: 72.8 us
  Pallas kernels  71.4 us (98%)
  local copies, waits for them, and re-layouts  1.32 us (2%)
    pallas_call x1, Pallas kernels, shards(): pl.pallas_call(functools.partial(kernel, layers, peers), out_shape=jax.Sh...  71.4 us

profile of v2, /device:TPU:1, one launch (start us, length us, event | category | flops | bytes accessed | tf_op | source)
XLA Modules:
  0.0 72.8 jit_solution(10931758817145352003)
XLA Ops:
  0.0 71.4 %shard_map.100 = bf16[512,2048]{1,0:T(8,128)(2,1)S(1)} custom-call(bf16[512,2048]{1,0:T(8,128)(2,1)} %tokens.1, f32[1,2048]{1,0:T(1,128)} %bitcast.3, bf16[128,512]{1,0:T(8,128)(2,1)} %wq.1, bf16[128,512]{1,0:T(8,128)(2,1)} %wk.1, bf16[128,512]{1,0:T(8,128)(2,1)} %wv.1, bf16[512,128]{1,0:T(8,128)(2,1)} %wo.1, f32[4,8]{1,0:T(4,128)} %bitcast.4, ...), custom_call_target="tpu_custom_call" | custom-call | tf_op jit(solution)/shard_map/pallas_call | solution.py:654
  71.4 1.3 %copy.12 = bf16[512,2048]{1,0:T(8,128)(2,1)} copy(bf16[512,2048]{1,0:T(8,128)(2,1)S(1)} %shard_map.100) | data formatting | bytes 4194304

commit v3 on v2

--- a/solution.py
+++ b/solution.py
@@ -29,7 +29,7 @@
         self.pieces = (0, 1) if split else (None,)
         self.z, self.y, self.x, self.tp = place
         self.rows = buf.shape[0] // (4 * layers)
-        self.r_x, self.r_y, self.r_z, self.r_w, self.sent = sems
+        self.got, self.r_z, self.sent = sems
         self.inner = (self.z > 0) & (self.z < layers - 1)
 
     def at(self, zi, yi, xi, piece=None):
@@ -52,18 +52,23 @@
 
     def copy_x(self, t, j):
         ref = self.at(self.layer(t), 1 - self.y if j == 2 else self.y, self.x, (0, 1, 0, None)[j])
-        return remote(ref, ref, self.sent.at[0], self.r_x.at[t // 2, j],
+        return remote(ref, ref, self.sent.at[0], self.got.at[t // 2, (4, 0, 2, 5)[j]],
                       self.device(self.z, self.y, 1 - self.x))
 
     def copy_y(self, t, j):
         ref = self.at(self.layer(t), self.y, 1 - self.x if j == 2 else self.x, (1, 0, 1, None)[j])
-        return remote(ref, ref, self.sent.at[0], self.r_y.at[t // 2, j],
+        return remote(ref, ref, self.sent.at[0], self.got.at[t // 2, (4, 1, 3, 5)[j]],
                       self.device(self.z, 1 - self.y, self.x))
 
     def copy_w(self, t, j):
         ref = self.at(self.layer(t), 1 - self.y, 1 - self.x, j)
-        return remote(ref, ref, self.sent.at[0], self.r_w.at[t // 2, j],
+        return remote(ref, ref, self.sent.at[0], self.got.at[t // 2, 5],
                       self.device(self.layer(1), self.y, self.x))
+
+    def whole(self, t, shards, k):
+        ref = self.buf.at[pl.ds(0, shards * self.rows)]
+        remote(ref, ref, self.sent.at[0], self.got.at[t // 2, k],
+               self.device(self.z, self.y, 1 - self.x)).wait_recv()
 
     def copy_z(self, zi, step, piece):
         ref = self.at(zi, self.y, self.x, piece)
@@ -161,14 +166,7 @@
         self.copy_w(t, 1).start()
 
     def arrive(self, t):
-        if t % 2:
-            self.copy_x(t, 3).wait_recv()
-            self.copy_y(t, 3).wait_recv()
-            self.copy_w(t - 1, 0).wait_recv()
-            self.copy_w(t - 1, 1).wait_recv()
-        else:
-            self.copy_x(t, 0).wait_recv()
-            self.copy_y(t, 0).wait_recv()
+        self.whole(t, 3, 5) if t % 2 else self.whole(t, 1, 4)
         return self.layer(t)
 
     def drain(self):
@@ -193,7 +191,7 @@
 
 
 def kernel(layers, peers, tokens, gain_in, wq, wk, wv, wo, rates_in, state_in, out_gain_in, freq_in, out,
-           gain, rates, state_init, out_gain, freq, small_sem, wkv_all, wq_all, wo_all, wo_own, toks, normed, acc, cosine, sine, q_rot, k_rot, v_row, weigh, inner,
+           gain, rates, state_init, out_gain, freq, small_sem, wkv_all, wq_all, wo_all, wo_own, toks, normed, acc, cosine, sine, q_rot, k_rot, v_row, weigh,
            prev, state, hidden, part, landed, tot_send, tot_recv, excl, excl_d, pl_send, pl_recv,
            in_send, in_recv, start, incoming, local_sem, tok_sem, nrm_s, nrm_r, part_s, part_r, t_s, t_r,
            p_s, p_r, i_s, i_r,
@@ -207,10 +205,10 @@
     blocks = span // BLOCK
     shard = wq.shape[0]
     place = (z, y, x, tp)
-    gk = Gather(wkv_all, layers, place, gather_sems[:5], True)
-    gq = Gather(wq_all, layers, place, gather_sems[5:10])
-    go = Gather(wo_all, layers, place, gather_sems[10:])
-    parts = nrm_s.shape[1]
+    gk = Gather(wkv_all, layers, place, gather_sems[:3], True)
+    gq = Gather(wq_all, layers, place, gather_sems[3:6])
+    go = Gather(wo_all, layers, place, gather_sems[6:])
+    parts = tok_sem.shape[0]
     chunk = rows_here // parts
 
     mine = pl.ds(pl.multiple_of(me * shard, shard), shard)
@@ -264,10 +262,14 @@
 
     def send_normed(d, c):
         ref = normed.at[pl.ds(pl.multiple_of(base + c * chunk, chunk), chunk)]
-        return remote(ref, ref, nrm_s.at[d - 1, c], nrm_r.at[d - 1, c], (me, (tp + d) % peers))
+        return remote(ref, ref, nrm_s.at[d - 1], nrm_r.at[d - 1], (me, (tp + d) % peers))
 
     for copy in smalls:
         copy.wait()
+    def sent_normed(d):
+        ref = normed.at[pl.ds(base, rows_here)]
+        return remote(ref, ref, nrm_s.at[d - 1], nrm_r.at[d - 1], (me, (tp + d) % peers))
+
     for c in range(parts):
         loads[c].wait()
 
@@ -355,7 +357,7 @@
         return (4 * z + toward(r), tp)
 
     def total_to(r, i):
-        return remote(tot_send.at[4 * i + toward(r)], tot_recv.at[i, r], t_s.at[i, r], t_r.at[i, r], beside(r))
+        return remote(tot_send.at[4 * i + toward(r)], tot_recv.at[i, r], t_s.at[i], t_r.at[i], beside(r))
 
     def plane_to(k, i):
         return remote(pl_send.at[i], pl_recv.at[i, z], p_s.at[i, k], p_r.at[i, z], (4 * (z + k) + corner, tp))
@@ -364,7 +366,10 @@
         return remote(pl_send.at[i], pl_recv.at[i, zz], p_s.at[i, 0], p_r.at[i, zz], (4 * z + corner, tp))
 
     def start_to(r, i):
-        return remote(in_send.at[i, r], in_recv.at[i, r], i_s.at[i, r], i_r.at[i, r], beside(r))
+        return remote(in_send.at[i, r], in_recv.at[i, r], i_s.at[i], i_r.at[i], beside(r))
+
+    def all_three(ref, send, recv):
+        return remote(ref, ref, send, recv, beside(1))
 
     def packed(decay, value):
         return jnp.concatenate([value, jnp.broadcast_to(decay, (16, HEAD_DIM))], axis=0).astype(BF16)
@@ -388,8 +393,7 @@
         def act():
             for i in range(slots):
                 tot_recv[i, 0] = tot_send[4 * i + corner]
-                for r in (1, 2, 3):
-                    total_to(r, i).wait_recv()
+                all_three(tot_recv.at[i, pl.ds(1, 3)], t_s.at[i], t_r.at[i]).wait_recv()
                 decay, value = jnp.ones((1, HEAD_DIM), F32), jnp.zeros((HEAD_DIM, HEAD_DIM), F32)
                 for j in range(4):
                     excl[i, j], excl_d[i, j] = value, jnp.broadcast_to(decay, (8, HEAD_DIM))
@@ -421,73 +425,86 @@
 
     def started():
         for i in range(slots):
+            if heads >= 4:
+                all_three(in_recv.at[i, pl.ds(1, 3)], i_s.at[i], i_r.at[i]).wait_recv()
             for r in (1, 2, 3):
                 def act():
-                    start_to(r, i).wait_recv()
+                    if heads < 4:
+                        start_to(r, i).wait_recv()
                     incoming[4 * i + toward(r)] = in_recv[i, r].astype(F32)
                 guard(r, act)
 
     def sent_states():
         for i in range(slots):
-            for r in (1, 2, 3):
-                guard(r, total_to(r, i).wait_send)
+            if heads >= 4:
+                all_three(tot_recv.at[i, pl.ds(1, 3)], t_s.at[i], t_r.at[i]).wait_send()
+            else:
+                for r in (1, 2, 3):
+                    guard(r, total_to(r, i).wait_send)
 
             def act():
-                for r in (1, 2, 3):
-                    start_to(r, i).wait_send()
+                all_three(in_recv.at[i, pl.ds(1, 3)], i_s.at[i], i_r.at[i]).wait_send()
                 for k in range(1, layers):
                     pl.when(z + k < layers)(plane_to(k, i).wait_send)
             mine_only(act)
 
-    def turn(b, carry):
-        at = pl.ds(pl.multiple_of(b * BLOCK, BLOCK), BLOCK)
-        cos, sin = cosine[at, :], sine[at, :]
-        for h in range(heads):
-            head = pl.ds(h * HEAD_DIM, HEAD_DIM)
-            u = acc[at, head]
-            q_rot[at, head] = (u * cos + pltpu.roll(u, HEAD_DIM // 2, 1) * sin).astype(BF16)
-        return carry
-
-    def scores(b):
+    def turned(t):
+        with SCOPE("arrive"):
+            zi = gq.arrive(t)
+        at_k = pl.ds(pl.multiple_of(zi * deep, deep), deep)
+        with SCOPE("turned"):
+            @pl.loop(0, span // m_tile)
+            def _(i):
+                at = pl.ds(pl.multiple_of(i * m_tile, m_tile), m_tile)
+                u_all = acc[at, :cols] + jnp.dot(
+                    normed[at, at_k], gq.buf[at_k, :], preferred_element_type=F32)
+                cos, sin = cosine[at, :], sine[at, :]
+                for h in range(heads):
+                    u = u_all[:, h * HEAD_DIM:(h + 1) * HEAD_DIM]
+                    q = u * cos + pltpu.roll(u, HEAD_DIM // 2, 1) * sin
+                    q_rot[at, h * HEAD_DIM:(h + 1) * HEAD_DIM] = q.astype(BF16)
+                    for n in range(m_tile // BLOCK):
+                        read = jnp.exp(-(row + 1.0) * rates[h, i * (m_tile // BLOCK) + n])
+                        at_b = pl.ds(pl.multiple_of(i * m_tile + n * BLOCK, BLOCK), BLOCK)
+                        weigh[at_b, (2 * h + 1) * HEAD_DIM:(2 * h + 2) * HEAD_DIM] = (
+                            q[n * BLOCK:(n + 1) * BLOCK] * read).astype(BF16)
+
+    def scores(b, carry):
         at = pl.ds(pl.multiple_of(b * BLOCK, BLOCK), BLOCK)
         for h in range(heads):
             head = pl.ds(h * HEAD_DIM, HEAD_DIM)
             fall = jnp.where(gap >= 0.0, jnp.exp(-jnp.maximum(gap, 0.0) * rates[h, b]), 0.0)
             score = nt_dot(q_rot[at, head], k_rot[at, head]) * (fall * HEAD_DIM ** (-0.5))
-            weigh[at, head] = score.astype(BF16)
-
-    def gathered(b):
-        at = pl.ds(pl.multiple_of(b * BLOCK, BLOCK), BLOCK)
-        for h in range(heads):
-            head = pl.ds(h * HEAD_DIM, HEAD_DIM)
-            inner[at, head] = jnp.dot(weigh[at, head], v_row[at, head], preferred_element_type=F32)
-
-    def inside(b, carry):
-        gathered(b - 1)
-        scores(b)
+            weigh[at, 2 * h * HEAD_DIM:(2 * h + 1) * HEAD_DIM] = score.astype(BF16)
         return carry
 
     def finish(b, sums):
         at = pl.ds(pl.multiple_of(b * BLOCK, BLOCK), BLOCK)
         new = []
         for h in range(heads):
-            rate = rates[h, b]
             head = pl.ds(h * HEAD_DIM, HEAD_DIM)
             before = prev[b, h] + decay_of(sums[h]) * incoming[h]
-            read = jnp.exp(-(row + 1.0) * rate)
-            kept = inner[at, head] + read * jnp.dot(
-                q_rot[at, head], before.astype(BF16), preferred_element_type=F32)
+            kept = jnp.dot(weigh[at, 2 * h * HEAD_DIM:(2 * h + 2) * HEAD_DIM],
+                           jnp.concatenate([v_row[at, head], before.astype(BF16)], axis=0),
+                           preferred_element_type=F32)
             kept = kept * lax.rsqrt(jnp.mean(kept * kept, axis=-1, keepdims=True) + EPS)
             hidden[at, head] = (kept * out_gain[:, head]).astype(BF16)
-            new.append(sums[h] + rate)
+            new.append(sums[h] + rates[h, b])
         return tuple(new)
 
     wide = 4 * out_shard
-    o_tile = min(512, rows_here)
-
-    def hand(d, t):
-        return remote(part.at[d - 1, t], landed.at[d - 1, t], part_s.at[d - 1, t], part_r.at[d - 1, t],
-                      (me, (tp + d) % peers))
+
+    half_rows = rows_here // 2
+
+    def hand(d, t, part_no=None):
+        src, dst, k = part.at[d - 1, t], landed.at[d - 1, t], 2 * t
+        if part_no is not None:
+            rows = pl.ds(part_no * half_rows, half_rows)
+            src, dst, k = src.at[rows], dst.at[rows], 2 * t + part_no
+        return remote(src, dst, part_s.at[d - 1], part_r.at[d - 1, k], (me, (tp + d) % peers))
+
+    def handed(t):
+        return (0, 1) if t % 2 else (None,)
 
     def pieces(t):
         with SCOPE("oarrive"):
@@ -497,26 +514,25 @@
     def theirs(t):
         rows_o = pieces(t)
         with SCOPE("theirs"):
-            for d in range(1, peers):
-                @pl.loop(0, rows_here // o_tile)
-                def _(i):
-                    start = ((tp + d) % peers) * rows_here
-                    rows = pl.ds(pl.multiple_of(start + i * o_tile, o_tile), o_tile)
-                    part[d - 1, t, pl.ds(pl.multiple_of(i * o_tile, o_tile), o_tile), :] = nt_dot(
+            for n in handed(t):
+                count = rows_here if n is None else half_rows
+                for d in range(1, peers):
+                    start = ((tp + d) % peers) * rows_here + (n or 0) * half_rows
+                    rows = pl.ds(pl.multiple_of(start, count), count)
+                    part[d - 1, t, pl.ds((n or 0) * half_rows, count), :] = nt_dot(
                         hidden[rows, :], wo_all[rows_o, :]).astype(BF16)
-
-                hand(d, t).start()
+                    hand(d, t, n).start()
 
     def ours(t):
         at_c = pl.ds(pl.multiple_of(go.layer(t) * wide, wide), wide)
-        with SCOPE("w_hand"):
-            for d in range(1, peers):
-                hand(d, t).wait_recv()
-        with SCOPE("ours"):
-            @pl.loop(0, rows_here // o_tile)
-            def _(i):
-                at = pl.ds(pl.multiple_of(i * o_tile, o_tile), o_tile)
-                rows = pl.ds(pl.multiple_of(base + i * o_tile, o_tile), o_tile)
+        for n in handed(t):
+            count = rows_here if n is None else half_rows
+            with SCOPE("w_hand"):
+                for d in range(1, peers):
+                    hand(d, t, n).wait_recv()
+            with SCOPE("ours"):
+                at = pl.ds((n or 0) * half_rows, count)
+                rows = pl.ds(pl.multiple_of(base + (n or 0) * half_rows, count), count)
                 value = nt_dot(hidden[rows, :], wo_all[at_c, :])
                 for d in range(1, peers):
                     value = value + landed[d - 1, t, at, :].astype(F32)
@@ -541,8 +557,7 @@
     sc("trig", lambda: lax.fori_loop(cut, blocks, trig, 0))
     with SCOPE("nrmwait"):
         for d in range(1, peers):
-            for c in range(parts):
-                send_normed(d, c).wait_recv()
+            sent_normed(d).wait_recv()
     sc("kstage2a", gk.stage, 2, (0,))
     sc("kstage2b", gk.stage, 2, (1,))
     each("kspread", evens, gk.spread)
@@ -565,6 +580,7 @@
         product(gk, t, 1, 1, 2)
     sc("qcross0", gq.cross, 0)
     go.lead(False)
+    go.spread(0)
     product(gk, last, 1, 1, 2)
 
     for h in range(heads):
@@ -581,54 +597,54 @@
     sc("qouter1", gq.outer, 1)
     each("qspread", odds, gq.spread)
     gq.spread(last)
+    product(gq, 0, 1, 0, 1)
     each("qswap2", evens, gq.swap)
     sc("plane_tot", plane_totals)
     sc("omiddle3", go.middle, 3)
+    sc("oouter2", go.outer, 2)
     go.lead(True)
-    go.spread(0)
-    product(gq, 0, 2, 0, 1)
-    sc("oouter2", go.outer, 2)
     each("ospread", evens, go.spread)
+    sc("ocross0", go.cross, 0)
+    for t in evens:
+        product(gq, t, 1, 0, 1)
+    for t in odds:
+        product(gq, t, 1, 0, 1)
     sc("starts", starts)
-    for t in evens:
-        product(gq, t, 2, 0, 1)
-    sc("ocross0", go.cross, 0)
-    with SCOPE("turn"):
-        lax.fori_loop(0, blocks, turn, 0)
-    scores(0)
+    turned(last)
+    each("ocross2", evens, go.cross)
     sc("oouter3", go.outer, 3)
     go.spread(last)
-    each("ocross2", evens, go.cross)
-    with SCOPE("inside"):
-        lax.fori_loop(1, cut, inside, 0)
+    with SCOPE("scores"):
+        lax.fori_loop(0, cut, scores, 0)
     sc("oouter1", go.outer, 1)
     each("ospread", odds, go.spread)
     sc("oswap0", go.swap, 0)
-    with SCOPE("inside"):
-        lax.fori_loop(cut, blocks, inside, 0)
-        gathered(blocks - 1)
+    with SCOPE("scores"):
+        lax.fori_loop(cut, blocks, scores, 0)
     sc("started", started)
     with SCOPE("finish"):
         sums = lax.fori_loop(0, cut, finish, (jnp.float32(0.0),) * heads)
     each("oswap2", evens, go.swap)
     with SCOPE("finish"):
         lax.fori_loop(cut, blocks, finish, sums)
-    turns = (0,) + tuple(evens) + tuple(odds) + (last,) if layers > 2 else (0, 1)
-    for i in range(layers + 2):
-        if i < layers:
-            theirs(turns[i])
-        if i >= 2:
-            ours(turns[i - 2])
+    first, rest = (0,) + tuple(evens), tuple(odds) + (last,)
+
+    def project(order):
+        for turn, fn in order:
+            for t in turn:
+                fn(t)
+
+    pl.when(tp % 2 == 0)(lambda: project(((first, theirs), (first, ours), (rest, theirs), (rest, ours))))
+    pl.when(tp % 2 == 1)(lambda: project(((first, theirs), (rest, theirs), (first, ours), (rest, ours))))
 
     with SCOPE("drain"):
         gk.drain()
         gq.drain()
         go.drain()
         for d in range(1, peers):
-            for c in range(parts):
-                send_normed(d, c).wait_send()
-            for t in range(layers):
-                hand(d, t).wait_send()
+            sent_normed(d).wait_send()
+            remote(part.at[d - 1], landed.at[d - 1], part_s.at[d - 1], part_r.at[d - 1, 0],
+                   (me, (tp + d) % peers)).wait_send()
         sent_states()
 
 
@@ -649,7 +665,7 @@
     dma = pltpu.SemaphoreType.DMA
     others, slots = max(peers - 1, 1), max(heads // 4, 1)
     parts = 2
-    gather_sems = [dma((layers // 2, 4))] * 2 + [dma((layers, 2)), dma((layers // 2, 2)), dma((2,))]
+    gather_sems = [dma((layers // 2, 6)), dma((layers, 1)), dma((2,))]
     v = pltpu.VMEM
     return pl.pallas_call(
         functools.partial(kernel, layers, peers),
@@ -663,8 +679,8 @@
             v(w_out.shape, BF16), v((rows_here, width), BF16),
             v((span, width), BF16),
             v((span, 3 * cols), F32), v((span, HEAD_DIM), F32), v((span, HEAD_DIM), F32),
-            v((span, cols), BF16), v((span, cols), BF16), v((span, cols), BF16), v((span, cols), BF16),
-            v((span, cols), F32), v((blocks, heads, HEAD_DIM, HEAD_DIM), F32),
+            v((span, cols), BF16), v((span, cols), BF16), v((span, cols), BF16), v((span, 2 * cols), BF16),
+            v((blocks, heads, HEAD_DIM, HEAD_DIM), F32),
             v((heads, HEAD_DIM, HEAD_DIM), F32), v((span, cols), BF16),
             v((others, layers, rows_here, wide), BF16), v((others, layers, rows_here, wide), BF16),
             v((heads, HEAD_DIM + 16, HEAD_DIM), BF16), v((slots, 4, HEAD_DIM + 16, HEAD_DIM), BF16),
@@ -672,11 +688,11 @@
             v((slots, HEAD_DIM + 16, HEAD_DIM), BF16), v((slots, layers, HEAD_DIM + 16, HEAD_DIM), BF16),
             v((slots, 4, HEAD_DIM, HEAD_DIM), BF16), v((slots, 4, HEAD_DIM, HEAD_DIM), BF16),
             v((HEAD_DIM, HEAD_DIM), F32), v((heads, HEAD_DIM, HEAD_DIM), F32),
-            dma((4,)), dma((parts,)), dma((others, parts)), dma((others, parts)),
-            dma((others, layers)), dma((others, layers)),
-            dma((slots, 4)), dma((slots, 4)), dma((slots, layers)), dma((slots, layers)),
-            dma((slots, 4)), dma((slots, 4)),
-        ] + gather_sems * 3,
+            dma((4,)), dma((parts,)), dma((others,)), dma((others,)),
+            dma((others,)), dma((others, 2 * layers)),
+            dma((slots,)), dma((slots,)), dma((slots, layers)), dma((slots, layers)),
+            dma((slots,)), dma((slots,)),
+        ] + [gather_sems[0], dma((layers, 2)), gather_sems[2]] + gather_sems * 2,
         compiler_params=pltpu.CompilerParams(
             collective_id=0, has_side_effects=True, vmem_limit_bytes=46 * 1024 * 1024),
     )(*(pltpu.with_memory_space_constraint(u, pltpu.HBM) for u in (

time: 73.1 us -> 69.3 us (0.948)
  Pallas kernels: 71.4 us -> 67.8 us
    pallas_call x1, Pallas kernels: 71.4 us -> 67.8 us  [shards(): pl.pallas_call(functools.partial(kernel, layers, peers), out_shape=jax.Sh...]
where the time goes in v3:
time: 69.3 us; the launch traced here: 69.1 us
  Pallas kernels  67.8 us (98%)
  local copies, waits for them, and re-layouts  1.32 us (2%)
    pallas_call x1, Pallas kernels, shards(): pl.pallas_call(functools.partial(kernel, layers, peers), out_shape=jax.Sh...  67.8 us

profile of v3, /device:TPU:1, one launch (start us, length us, event | category | flops | bytes accessed | tf_op | source)
XLA Modules:
  0.0 69.1 jit_solution(4293782501734165626)
XLA Ops:
  0.0 67.8 %shard_map.100 = bf16[512,2048]{1,0:T(8,128)(2,1)S(1)} custom-call(bf16[512,2048]{1,0:T(8,128)(2,1)} %tokens.1, f32[1,2048]{1,0:T(1,128)} %bitcast.3, bf16[128,512]{1,0:T(8,128)(2,1)} %wq.1, bf16[128,512]{1,0:T(8,128)(2,1)} %wk.1, bf16[128,512]{1,0:T(8,128)(2,1)} %wv.1, bf16[512,128]{1,0:T(8,128)(2,1)} %wo.1, f32[4,8]{1,0:T(4,128)} %bitcast.4, ...), custom_call_target="tpu_custom_call" | custom-call | tf_op jit(solution)/shard_map/pallas_call | solution.py:670
  67.8 1.3 %copy.12 = bf16[512,2048]{1,0:T(8,128)(2,1)} copy(bf16[512,2048]{1,0:T(8,128)(2,1)S(1)} %shard_map.100) | data formatting | bytes 4194304

commit v4 on v3

--- a/solution.py
+++ b/solution.py
@@ -52,17 +52,17 @@
 
     def copy_x(self, t, j):
         ref = self.at(self.layer(t), 1 - self.y if j == 2 else self.y, self.x, (0, 1, 0, None)[j])
-        return remote(ref, ref, self.sent.at[0], self.got.at[t // 2, (4, 0, 2, 5)[j]],
+        return remote(ref, ref, self.sent.at[0], self.got.at[t // 2, (2, 0, 1, 3)[j]],
                       self.device(self.z, self.y, 1 - self.x))
 
     def copy_y(self, t, j):
         ref = self.at(self.layer(t), self.y, 1 - self.x if j == 2 else self.x, (1, 0, 1, None)[j])
-        return remote(ref, ref, self.sent.at[0], self.got.at[t // 2, (4, 1, 3, 5)[j]],
+        return remote(ref, ref, self.sent.at[0], self.got.at[t // 2, (2, 0, 1, 3)[j]],
                       self.device(self.z, 1 - self.y, self.x))
 
-    def copy_w(self, t, j):
-        ref = self.at(self.layer(t), 1 - self.y, 1 - self.x, j)
-        return remote(ref, ref, self.sent.at[0], self.got.at[t // 2, 5],
+    def copy_w(self, t):
+        ref = self.at(self.layer(t), 1 - self.y, 1 - self.x)
+        return remote(ref, ref, self.sent.at[0], self.got.at[t // 2, 4],
                       self.device(self.layer(1), self.y, self.x))
 
     def whole(self, t, shards, k):
@@ -154,19 +154,26 @@
         self.copy_y(t, 0).start()
 
     def cross(self, t):
-        self.copy_y(t, 1).wait_recv()
+        self.whole(t, 1, 0)
         self.copy_x(t, 2).start()
-        self.copy_x(t, 1).wait_recv()
         self.copy_y(t, 2).start()
 
     def swap(self, t):
-        self.copy_x(t, 2).wait_recv()
-        self.copy_w(t, 0).start()
-        self.copy_y(t, 2).wait_recv()
-        self.copy_w(t, 1).start()
+        self.whole(t, 1, 1)
+        self.copy_w(t).start()
+
+    def beside(self, t):
+        self.whole(t, 2, 3)
+
+    def across(self, t):
+        self.whole(t, 1, 4)
 
     def arrive(self, t):
-        self.whole(t, 3, 5) if t % 2 else self.whole(t, 1, 4)
+        if t % 2:
+            self.beside(t)
+            self.across(t)
+        else:
+            self.whole(t, 1, 2)
         return self.layer(t)
 
     def drain(self):
@@ -192,8 +199,8 @@
 
 def kernel(layers, peers, tokens, gain_in, wq, wk, wv, wo, rates_in, state_in, out_gain_in, freq_in, out,
            gain, rates, state_init, out_gain, freq, small_sem, wkv_all, wq_all, wo_all, wo_own, toks, normed, acc, cosine, sine, q_rot, k_rot, v_row, weigh,
-           prev, state, hidden, part, landed, tot_send, tot_recv, excl, excl_d, pl_send, pl_recv,
-           in_send, in_recv, start, incoming, local_sem, tok_sem, nrm_s, nrm_r, part_s, part_r, t_s, t_r,
+           prev, state, hidden, cum, hid_peer, wo_peer, begun, tot_send, tot_recv, excl, excl_d, pl_send, pl_recv,
+           in_send, in_recv, start, incoming, local_sem, tok_sem, nrm_s, nrm_r, hid_s, hid_r, wgt_s, wgt_r, t_s, t_r,
            p_s, p_r, i_s, i_r,
            *gather_sems):
     me, tp = lax.axis_index("sp"), lax.axis_index("tp")
@@ -232,6 +239,8 @@
             (gain_in, gain), (freq_in, freq), (rates_in, rates), (out_gain_in, out_gain),
             (state_in, state_init)))
     ]
+    for copy in fills[:2]:
+        copy.start()
     barrier = pltpu.get_barrier_semaphore()
 
     def greet(device):
@@ -244,11 +253,11 @@
     pl.when(z > 0)(lambda: greet(gq.device(z - 1, y, x)))
     pl.when(z < layers - 1)(lambda: greet(gq.device(z + 1, y, x)))
 
-    for copy in fills + loads + smalls:
+    for copy in fills[2:] + loads + smalls:
         copy.start()
 
     out_shard = wo.shape[1]
-    for fill in fills[:3]:
+    for fill in fills[:2]:
         fill.wait()
     with SCOPE("barrier"):
         pl.semaphore_wait(
@@ -285,7 +294,8 @@
         for d in range(1, peers):
             send_normed(d, c).start()
 
-    fills[3].wait()
+    for fill in fills[2:]:
+        fill.wait()
     wo_all[pl.ds(pl.multiple_of(me * out_shard, out_shard), out_shard), :] = wo_own[...].T
 
     def trig(i, carry):
@@ -337,6 +347,7 @@
             now = state[h]
             prev[b, h] = now
             state[h] = jnp.exp(jnp.full((1, HEAD_DIM), -float(BLOCK), F32) * rate) * now + kv
+            cum[h, b] = sums[h]
             new.append(sums[h] + rate)
         return tuple(new)
 
@@ -360,10 +371,10 @@
         return remote(tot_send.at[4 * i + toward(r)], tot_recv.at[i, r], t_s.at[i], t_r.at[i], beside(r))
 
     def plane_to(k, i):
-        return remote(pl_send.at[i], pl_recv.at[i, z], p_s.at[i, k], p_r.at[i, z], (4 * (z + k) + corner, tp))
+        return remote(pl_send.at[i], pl_recv.at[i, z], p_s.at[i], p_r.at[i, z], (4 * (z + k) + corner, tp))
 
     def plane_from(zz, i):
-        return remote(pl_send.at[i], pl_recv.at[i, zz], p_s.at[i, 0], p_r.at[i, zz], (4 * z + corner, tp))
+        return remote(pl_send.at[i], pl_recv.at[i, zz], p_s.at[i], p_r.at[i, zz], (4 * z + corner, tp))
 
     def start_to(r, i):
         return remote(in_send.at[i, r], in_recv.at[i, r], i_s.at[i], i_r.at[i], beside(r))
@@ -444,8 +455,9 @@
 
             def act():
                 all_three(in_recv.at[i, pl.ds(1, 3)], i_s.at[i], i_r.at[i]).wait_send()
-                for k in range(1, layers):
-                    pl.when(z + k < layers)(plane_to(k, i).wait_send)
+                for zz in range(layers - 1):
+                    ref = pl_recv.at[i, pl.ds(0, layers - 1 - zz)]
+                    pl.when(z == zz)(all_three(ref, p_s.at[i], p_r.at[i, 0]).wait_send)
             mine_only(act)
 
     def turned(t):
@@ -478,65 +490,94 @@
             weigh[at, 2 * h * HEAD_DIM:(2 * h + 1) * HEAD_DIM] = score.astype(BF16)
         return carry
 
-    def finish(b, sums):
+    def finish(b, carry):
         at = pl.ds(pl.multiple_of(b * BLOCK, BLOCK), BLOCK)
-        new = []
         for h in range(heads):
             head = pl.ds(h * HEAD_DIM, HEAD_DIM)
-            before = prev[b, h] + decay_of(sums[h]) * incoming[h]
+            before = prev[b, h] + decay_of(cum[h, b]) * incoming[h]
             kept = jnp.dot(weigh[at, 2 * h * HEAD_DIM:(2 * h + 2) * HEAD_DIM],
                            jnp.concatenate([v_row[at, head], before.astype(BF16)], axis=0),
                            preferred_element_type=F32)
             kept = kept * lax.rsqrt(jnp.mean(kept * kept, axis=-1, keepdims=True) + EPS)
             hidden[at, head] = (kept * out_gain[:, head]).astype(BF16)
-            new.append(sums[h] + rates[h, b])
-        return tuple(new)
+        return carry
+
+    def finish_rows(owner_tp):
+        start = owner_tp * (rows_here // BLOCK)
+        lax.fori_loop(start, start + rows_here // BLOCK, finish, 0)
 
     wide = 4 * out_shard
 
-    half_rows = rows_here // 2
-
-    def hand(d, t, part_no=None):
-        src, dst, k = part.at[d - 1, t], landed.at[d - 1, t], 2 * t
-        if part_no is not None:
-            rows = pl.ds(part_no * half_rows, half_rows)
-            src, dst, k = src.at[rows], dst.at[rows], 2 * t + part_no
-        return remote(src, dst, part_s.at[d - 1], part_r.at[d - 1, k], (me, (tp + d) % peers))
-
-    def handed(t):
-        return (0, 1) if t % 2 else (None,)
-
-    def pieces(t):
+    def columns(t):
+        return pl.ds(pl.multiple_of(go.layer(t) * wide, wide), wide)
+
+    def give_hidden(d):
+        rows = pl.ds(pl.multiple_of(((tp + d) % peers) * rows_here, rows_here), rows_here)
+        return remote(hidden.at[rows], hid_peer.at[d - 1], hid_s.at[d - 1], hid_r.at[d - 1],
+                      (me, (tp + d) % peers))
+
+    def give_weight(d, t):
+        return remote(wo_all.at[columns(t)], wo_peer.at[d - 1, columns(t)], wgt_s.at[d - 1],
+                      wgt_r.at[d - 1, t], (me, (tp + d) % peers))
+
+    def forward(t):
         with SCOPE("oarrive"):
-            zi = go.arrive(t)
-        return pl.ds(pl.multiple_of(zi * wide, wide), wide)
-
-    def theirs(t):
-        rows_o = pieces(t)
-        with SCOPE("theirs"):
-            for n in handed(t):
-                count = rows_here if n is None else half_rows
-                for d in range(1, peers):
-                    start = ((tp + d) % peers) * rows_here + (n or 0) * half_rows
-                    rows = pl.ds(pl.multiple_of(start, count), count)
-                    part[d - 1, t, pl.ds((n or 0) * half_rows, count), :] = nt_dot(
-                        hidden[rows, :], wo_all[rows_o, :]).astype(BF16)
-                    hand(d, t, n).start()
-
-    def ours(t):
-        at_c = pl.ds(pl.multiple_of(go.layer(t) * wide, wide), wide)
-        for n in handed(t):
-            count = rows_here if n is None else half_rows
-            with SCOPE("w_hand"):
-                for d in range(1, peers):
-                    hand(d, t, n).wait_recv()
-            with SCOPE("ours"):
-                at = pl.ds((n or 0) * half_rows, count)
-                rows = pl.ds(pl.multiple_of(base + (n or 0) * half_rows, count), count)
-                value = nt_dot(hidden[rows, :], wo_all[at_c, :])
-                for d in range(1, peers):
-                    value = value + landed[d - 1, t, at, :].astype(F32)
-                out[at, at_c] = value.astype(BF16)
+            go.arrive(t)
+        for d in range(1, peers):
+            give_weight(d, t).start()
+
+    def give_shards(t, *corners):
+        for yi, xi in corners:
+            start = pl.multiple_of((4 * go.layer(t) + 2 * yi + xi) * out_shard, out_shard)
+            rows = pl.ds(start, out_shard)
+            for d in range(1, peers):
+                remote(wo_all.at[rows], wo_peer.at[d - 1, rows], wgt_s.at[d - 1], wgt_r.at[d - 1, t],
+                       (me, (tp + d) % peers)).start()
+
+    def forward_own(t):
+        give_shards(t, (y, x))
+
+    def forward_beside(t):
+        with SCOPE("w_beside"):
+            go.beside(t)
+        give_shards(t, (y, 1 - x), (1 - y, x))
+
+    def forward_across(t):
+        with SCOPE("w_across"):
+            go.across(t)
+        give_shards(t, (1 - y, 1 - x))
+
+    def own_part(t):
+        return nt_dot(hidden[pl.ds(base, rows_here), :], wo_all[columns(t), :])
+
+    def peer_part(t, value):
+        for d in range(1, peers):
+            value = value + nt_dot(hid_peer[d - 1], wo_peer[d - 1, columns(t), :])
+        return value
+
+    def await_weight(t):
+        with SCOPE("w_weight"):
+            for d in range(1, peers):
+                give_weight(d, t).wait_recv()
+
+    def full(t):
+        await_weight(t)
+        with SCOPE("full"):
+            out[:, columns(t)] = peer_part(t, own_part(t)).astype(BF16)
+
+    def begin(t):
+        with SCOPE("begin"):
+            begun[t // 2] = own_part(t)
+
+    def end(t):
+        await_weight(t)
+        with SCOPE("end"):
+            out[:, columns(t)] = peer_part(t, begun[t // 2]).astype(BF16)
+
+    def await_hidden():
+        with SCOPE("w_hidden"):
+            for d in range(1, peers):
+                give_hidden(d).wait_recv()
 
     def sc(name, fn, *args):
         with SCOPE(name):
@@ -614,28 +655,54 @@
     each("ocross2", evens, go.cross)
     sc("oouter3", go.outer, 3)
     go.spread(last)
+    forward_own(last)
     with SCOPE("scores"):
         lax.fori_loop(0, cut, scores, 0)
     sc("oouter1", go.outer, 1)
     each("ospread", odds, go.spread)
+    each("ofwd", odds, forward_own)
     sc("oswap0", go.swap, 0)
+    forward(0)
     with SCOPE("scores"):
         lax.fori_loop(cut, blocks, scores, 0)
     sc("started", started)
     with SCOPE("finish"):
-        sums = lax.fori_loop(0, cut, finish, (jnp.float32(0.0),) * heads)
-    each("oswap2", evens, go.swap)
+        for d in range(1, peers):
+            finish_rows((tp + d) % peers)
+            give_hidden(d).start()
+    for t in evens:
+        sc("oswap2", go.swap, t)
+        forward(t)
     with SCOPE("finish"):
-        lax.fori_loop(cut, blocks, finish, sums)
+        finish_rows(tp)
     first, rest = (0,) + tuple(evens), tuple(odds) + (last,)
 
-    def project(order):
-        for turn, fn in order:
-            for t in turn:
+    def project(early):
+        def run(fn, ts):
+            for t in ts:
                 fn(t)
 
-    pl.when(tp % 2 == 0)(lambda: project(((first, theirs), (first, ours), (rest, theirs), (rest, ours))))
-    pl.when(tp % 2 == 1)(lambda: project(((first, theirs), (rest, theirs), (first, ours), (rest, ours))))
+        if early:
+            run(forward_beside, (last,))
+            run(forward_across, odds)
+            run(forward_beside, odds)
+            run(forward_across, (last,))
+        await_hidden()
+        run(full, (0,))
+        if not early:
+            run(forward_beside, (last,))
+            run(forward_across, odds)
+        run(full, evens)
+        if not early:
+            run(forward_beside, odds)
+        run(begin, odds)
+        if not early:
+            run(forward_across, (last,))
+        run(begin, (last,))
+        run(end, rest)
+
+    pl.when(tp % 2 == 0)(lambda: project(False))
+    pl.when(tp % 2 == 1)(lambda: project(True))
 
     with SCOPE("drain"):
         gk.drain()
@@ -643,7 +710,8 @@
         go.drain()
         for d in range(1, peers):
             sent_normed(d).wait_send()
-            remote(part.at[d - 1], landed.at[d - 1], part_s.at[d - 1], part_r.at[d - 1, 0],
+            give_hidden(d).wait_send()
+            remote(wo_all, wo_peer.at[d - 1], wgt_s.at[d - 1], wgt_r.at[d - 1, 0],
                    (me, (tp + d) % peers)).wait_send()
         sent_states()
 
@@ -665,7 +733,7 @@
     dma = pltpu.SemaphoreType.DMA
     others, slots = max(peers - 1, 1), max(heads // 4, 1)
     parts = 2
-    gather_sems = [dma((layers // 2, 6)), dma((layers, 1)), dma((2,))]
+    gather_sems = [dma((layers // 2, 5)), dma((layers, 1)), dma((2,))]
     v = pltpu.VMEM
     return pl.pallas_call(
         functools.partial(kernel, layers, peers),
@@ -682,15 +750,16 @@
             v((span, cols), BF16), v((span, cols), BF16), v((span, cols), BF16), v((span, 2 * cols), BF16),
             v((blocks, heads, HEAD_DIM, HEAD_DIM), F32),
             v((heads, HEAD_DIM, HEAD_DIM), F32), v((span, cols), BF16),
-            v((others, layers, rows_here, wide), BF16), v((others, layers, rows_here, wide), BF16),
+            pltpu.SMEM((heads, blocks), F32), v((others, rows_here, cols), BF16),
+            v((others, width, cols), BF16), v((layers // 2, rows_here, wide), F32),
             v((heads, HEAD_DIM + 16, HEAD_DIM), BF16), v((slots, 4, HEAD_DIM + 16, HEAD_DIM), BF16),
             v((slots, 4, HEAD_DIM, HEAD_DIM), F32), v((slots, 4, 8, HEAD_DIM), F32),
             v((slots, HEAD_DIM + 16, HEAD_DIM), BF16), v((slots, layers, HEAD_DIM + 16, HEAD_DIM), BF16),
             v((slots, 4, HEAD_DIM, HEAD_DIM), BF16), v((slots, 4, HEAD_DIM, HEAD_DIM), BF16),
             v((HEAD_DIM, HEAD_DIM), F32), v((heads, HEAD_DIM, HEAD_DIM), F32),
             dma((4,)), dma((parts,)), dma((others,)), dma((others,)),
-            dma((others,)), dma((others, 2 * layers)),
-            dma((slots,)), dma((slots,)), dma((slots, layers)), dma((slots, layers)),
+            dma((others,)), dma((others,)), dma((others,)), dma((others, layers)),
+            dma((slots,)), dma((slots,)), dma((slots,)), dma((slots, layers)),
             dma((slots,)), dma((slots,)),
         ] + [gather_sems[0], dma((layers, 2)), gather_sems[2]] + gather_sems * 2,
         compiler_params=pltpu.CompilerParams(

time: 69.3 us -> 68.3 us (0.986)
  Pallas kernels: 67.8 us -> 66.9 us
    pallas_call x1, Pallas kernels: 67.8 us -> 66.9 us  [shards(): pl.pallas_call(functools.partial(kernel, layers, peers), out_shape=jax.Sh...]
where the time goes in v4:
time: 68.3 us; the launch traced here: 68.2 us
  Pallas kernels  66.9 us (98%)
  local copies, waits for them, and re-layouts  1.32 us (2%)
    pallas_call x1, Pallas kernels, shards(): pl.pallas_call(functools.partial(kernel, layers, peers), out_shape=jax.Sh...  66.9 us

profile of v4, /device:TPU:1, one launch (start us, length us, event | category | flops | bytes accessed | tf_op | source)
XLA Modules:
  0.0 68.2 jit_solution(344968277601071281)
XLA Ops:
  0.0 66.9 %shard_map.100 = bf16[512,2048]{1,0:T(8,128)(2,1)S(1)} custom-call(bf16[512,2048]{1,0:T(8,128)(2,1)} %tokens.1, f32[1,2048]{1,0:T(1,128)} %bitcast.3, bf16[128,512]{1,0:T(8,128)(2,1)} %wq.1, bf16[128,512]{1,0:T(8,128)(2,1)} %wk.1, bf16[128,512]{1,0:T(8,128)(2,1)} %wv.1, bf16[512,128]{1,0:T(8,128)(2,1)} %wo.1, f32[4,8]{1,0:T(4,128)} %bitcast.4, ...), custom_call_target="tpu_custom_call" | custom-call | tf_op jit(solution)/shard_map/pallas_call | solution.py:738
  66.9 1.3 %copy.12 = bf16[512,2048]{1,0:T(8,128)(2,1)} copy(bf16[512,2048]{1,0:T(8,128)(2,1)S(1)} %shard_map.100) | data formatting | bytes 4194304
